TPU v7x, 256 devices: a whole 4x4x8 slice. The times are simulated.
256 devices in a mesh: sp: 32 (over z, x), tp: 8 (over y, core).
Axes of the slice: x: 4, y: 4, z: 8, core: 2. Of those that a mesh axis runs over, the one named last changes fastest.
Arguments:
- tokens: bfloat16 [16384, 2048], P(('sp', 'tp')), may hold values from -64 to 64
- query_weight: bfloat16 [2048, 2048], P(None, 'tp'), may hold values from -0.125 to 0.125
- key_weight: bfloat16 [2048, 2048], P(None, 'tp'), may hold values from -0.125 to 0.125
- value_weight: bfloat16 [2048, 2048], P(None, 'tp'), may hold values from -0.125 to 0.125
- gate_weight: bfloat16 [2048, 2048], P(None, 'tp'), may hold values from -0.125 to 0.125
- forget_weight: bfloat16 [2048, 16], replicated, may hold values from -0.125 to 0.125
- forget_bias: float32 [16], replicated, as said below
- out_weight: bfloat16 [2048, 2048], replicated, may hold values from -0.125 to 0.125
Outputs:
- mixed: bfloat16 [16384, 2048], P(('sp', 'tp'))
Inputs may be any that keep to these rules, and one draw needn't show every extreme that they name: `forget_bias`: every head's forget bias is at least 4.
All inputs are finite; a program needn't handle non-finite values.
Results may differ from a plain program's by a relative error of at most 0.015.
The roundings to bfloat16 on the way count: a program that leaves them out, or rounds other values in their place, can miss the bound.
Values may be sent and summed in bfloat16 or wider, within the bound.
No kernel may reach another device: no remote copies, remote signals or barrier semaphores. Data moves between devices by JAX's collectives and lax.ppermute only.
A program may use at most 128 MiB of HBM per device.

v0:
```python
import functools

import jax
import jax.numpy as jnp
from jax import lax
from jax.experimental import pallas as pl
from jax.experimental.pallas import tpu as pltpu
from jax.sharding import Mesh
from jax.sharding import PartitionSpec as P


HEAD_DIM = 128
NZ, NX, NY, NC = 8, 4, 4, 2
BLOCK = 512
HALF = 256
SLAB = NX * BLOCK
PIECE = 64
WIDTH = 2048
COLS = 256
META = 16
ROWS = 2 * HALF + META
NEG = -1e30

VMEM = pltpu.VMEM
SMEM = pltpu.SMEM
BF = jnp.bfloat16
F32 = jnp.float32


def vspec():
    return pl.BlockSpec(memory_space=VMEM)


def sspec():
    return pl.BlockSpec(memory_space=SMEM)


def thirds(value):
    high = value.astype(BF).astype(F32)
    rest = value - high
    mid = rest.astype(BF).astype(F32)
    low = (rest - mid).astype(BF).astype(F32)
    return high, mid, low


def gather(ids_ref, pieces, toks_ref, weights, sems):
    y, c = ids_ref[2], ids_ref[3]
    parts = 4
    pairs = []
    for source, target in weights:
        for i in range(parts):
            rows = pl.ds(i * WIDTH // parts, WIDTH // parts)
            pairs.append((source.at[rows, :], target.at[rows, :]))
    for i in range(8):
        pos = 2 * ((y + NY - i % NY) % NY) + (c if i < NY else 1 - c)
        start = pl.multiple_of(pos * PIECE, PIECE)
        pairs.append((pieces[i], toks_ref.at[pl.ds(start, PIECE), :]))
    copies = [
        pltpu.make_async_copy(source, target, sems.at[i])
        for i, (source, target) in enumerate(pairs)
    ]
    for copy in copies:
        copy.start()
    for copy in copies:
        copy.wait()
    return toks_ref[...]


def kv_kernel(ids_ref, *refs):
    wk_hbm, wv_hbm, fw_ref, bias_ref, kv_ref, toks_ref, wk_ref, wv_ref, sems, parts_ref = refs[8:]
    y, c = ids_ref[2], ids_ref[3]
    weights = [(wk_hbm, wk_ref), (wv_hbm, wv_ref)]
    toks = gather(ids_ref, refs[:8], toks_ref, weights, sems)
    keys = jnp.dot(toks, wk_ref[...], preferred_element_type=F32).astype(BF)
    values = jnp.dot(toks, wv_ref[...], preferred_element_type=F32).astype(BF)
    logits = lax.dot_general(
        fw_ref[...], toks, (((1,), (1,)), ((), ())), preferred_element_type=F32
    )
    row = lax.broadcasted_iota(jnp.int32, (16, BLOCK), 0)
    for head in range(16):
        logits = logits + jnp.where(row == head, bias_ref[head], 0.0)
    logs = jnp.minimum(logits, 0.0) - jnp.log1p(jnp.exp(-jnp.abs(logits)))
    row = lax.broadcasted_iota(jnp.int32, (BLOCK, BLOCK), 0)
    col = lax.broadcasted_iota(jnp.int32, (BLOCK, BLOCK), 1)
    upper = (row <= col).astype(BF)
    local = sum(
        jnp.dot(part.astype(BF), upper, preferred_element_type=F32) for part in thirds(logs)
    )
    for i, part in enumerate(thirds(local)):
        parts_ref[i] = part
    for a in range(2):
        head = 2 * (2 * y + c) + a
        mine = [parts_ref[i, pl.ds(head, 1), :] for i in range(3)]
        for b in range(2):
            dest = 2 * b + a
            rows = [
                part[:, b * HALF + i * 128 : b * HALF + (i + 1) * 128]
                for part in mine
                for i in range(2)
            ]
            rows += [jnp.broadcast_to(part[:, BLOCK - 1 :], (1, 128)) for part in mine]
            rows.append(jnp.zeros((META - 9, 128), F32))
            kv_ref[dest, :HALF, :] = keys[b * HALF : (b + 1) * HALF, a * 128 : (a + 1) * 128]
            kv_ref[dest, HALF : 2 * HALF, :] = values[
                b * HALF : (b + 1) * HALF, a * 128 : (a + 1) * 128
            ]
            kv_ref[dest, 2 * HALF :, :] = jnp.concatenate(rows, axis=0).astype(BF)


def query_kernel(ids_ref, *refs):
    wq_hbm, wg_hbm, qx_ref, gate_ref, toks_ref, wq_ref, wg_ref, sems = refs[8:]
    weights = [(wq_hbm, wq_ref), (wg_hbm, wg_ref)]
    toks = gather(ids_ref, refs[:8], toks_ref, weights, sems)
    queries = jnp.dot(toks, wq_ref[...], preferred_element_type=F32)
    queries = (queries * HEAD_DIM**-0.5).astype(BF)
    for b in range(2):
        for a in range(2):
            qx_ref[2 * b + a] = queries[:, a * 128 : (a + 1) * 128]
    pre = jnp.dot(toks, wg_ref[...], preferred_element_type=F32)
    gate = 1.0 / (1.0 + jnp.exp(-pre))
    for a in range(2):
        gate_ref[a] = gate[:, a * 128 : (a + 1) * 128]


def arrived_kernel(ids_ref, front_ref, back_ref, out_ref):
    for i in range(4):
        out_ref[i] = ids_ref[i]


QT = 256
KEYS = NX * HALF
TILES = SLAB // QT
ACC = 144


def fill(blocks, offsets, ka_ref, vt_ref):
    for j, ((ref, index), (rows, before)) in enumerate(zip(blocks, offsets)):
        ka_ref[j * HALF : (j + 1) * HALF, :128] = ref[index, :HALF, :]
        for g in range(2):
            cols = slice(j * HALF + g * 128, j * HALF + (g + 1) * 128)
            parts = thirds(-(rows[g] + before))
            tile = jnp.concatenate([*parts, jnp.zeros((125, 128), F32)], axis=0)
            ka_ref[cols, 128:] = tile.T.astype(BF)
            vals = ref[index, HALF + g * 128 : HALF + (g + 1) * 128, :]
            vt_ref[:128, cols] = vals.astype(F32).T.astype(BF)
    row = lax.broadcasted_iota(jnp.int32, (ACC - 128, KEYS), 0)
    vt_ref[128:, :] = jnp.where(row == 0, 1.0, 0.0).astype(BF)


def slab_offsets(blocks):
    out = []
    before = jnp.zeros((1, 128), F32)
    for ref, index in blocks:
        meta = ref[index, 2 * HALF :, :].astype(F32)
        rows = [meta[i : i + 1] + meta[2 + i : 3 + i] + meta[4 + i : 5 + i] for i in range(2)]
        out.append((rows, before))
        before = before + (meta[6:7] + meta[7:8] + meta[8:9])
    return out, before


def attend(qa_ref, ka_ref, vt_ref, half, old, new):
    m_out, acc_out = new

    def scores(i, keys):
        start = i * QT if half is not None else pl.multiple_of(i * QT, QT)
        s = lax.dot_general(
            ka_ref[:keys, :],
            qa_ref[pl.ds(start, QT), :],
            (((1,), (1,)), ((), ())),
            preferred_element_type=F32,
        )
        if half is not None:
            row = lax.broadcasted_iota(jnp.int32, (keys, QT), 0)
            col = lax.broadcasted_iota(jnp.int32, (keys, QT), 1)
            pos = row + (row // HALF + half) * HALF
            s = jnp.where(pos <= col + start, s, NEG)
        return s

    def finish(i, keys, s):
        best = jnp.max(s, axis=0, keepdims=True)
        if old is not None:
            before = old[0][i][:1]
            best = jnp.maximum(best, before)
        safe = jnp.where(best < -1e29, 0.0, best)
        w = jnp.exp(s - safe).astype(BF)
        acc = jnp.dot(vt_ref[:, :keys], w, preferred_element_type=F32)
        if old is not None:
            acc = acc + old[1][i] * jnp.exp(before - safe)
        m_out[i] = jnp.broadcast_to(best, (8, QT))
        acc_out[i] = acc

    def run(tiles):
        s = scores(*tiles[0])
        for tile, after in zip(tiles, [*tiles[1:], None]):
            following = scores(*after) if after else None
            finish(*tile, s)
            s = following

    if half is not None:
        run([(i, HALF * (i * QT // BLOCK + 1)) for i in range(TILES)])
    else:
        part = TILES // 2

        def some(j, carry):
            run([(j * part + i, KEYS) for i in range(part)])
            return carry

        lax.fori_loop(0, 2, some, 0)


def whole(ref):
    return [(ref, xs) for xs in range(NX)]


def diag_kernel(ids_ref, q_ref, kv_ref, qa_out, off_out, m_out, acc_out, ka_ref, vt_ref):
    offsets, _ = slab_offsets(whole(kv_ref))
    fill(whole(kv_ref), offsets, ka_ref, vt_ref)
    lane = lax.broadcasted_iota(jnp.int32, (SLAB, 128), 1)
    qa_out[:, :128] = q_ref[...]
    qa_out[:, 128:] = jnp.where(lane < 3, 1.0, 0.0).astype(BF)
    attend(qa_out, ka_ref, vt_ref, ids_ref[1] // 2, None, (m_out, acc_out))
    off_out[...] = jnp.zeros((8, 128), F32)


def shifted(offsets, base):
    return [(rows, before + base) for rows, before in offsets]


def front_kernel(
    step, ids_ref, qa_ref, kv_ref, off_in, m_in, acc_in, off_out, m_out, acc_out, ka_ref, vt_ref
):
    valid = ids_ref[0] >= step

    @pl.when(valid)
    def _():
        offsets, total = slab_offsets(whole(kv_ref))
        base = off_in[:1, :] - total
        fill(whole(kv_ref), shifted(offsets, base), ka_ref, vt_ref)
        attend(qa_ref, ka_ref, vt_ref, None, (m_in, acc_in), (m_out, acc_out))
        off_out[...] = jnp.broadcast_to(base, (8, 128))

    @pl.when(jnp.logical_not(valid))
    def _():
        off_out[...] = off_in[...]
        m_out[...] = m_in[...]
        acc_out[...] = acc_in[...]


def back_kernel(step, ids_ref, qa_ref, kv_ref, *refs):
    ins, (off_out, m_out, acc_out, ka_ref, vt_ref) = refs[:-5], refs[-5:]
    valid = ids_ref[0] + step >= NZ

    @pl.when(valid)
    def _():
        offsets, total = slab_offsets(whole(kv_ref))
        base = ins[0][:1, :] if ins else jnp.zeros((1, 128), F32)
        fill(whole(kv_ref), shifted(offsets, base), ka_ref, vt_ref)
        old = (ins[1], ins[2]) if ins else None
        attend(qa_ref, ka_ref, vt_ref, None, old, (m_out, acc_out))
        off_out[...] = jnp.broadcast_to(base + total, (8, 128))

    @pl.when(jnp.logical_not(valid))
    def _():
        if ins:
            off_out[...] = ins[0][...]
            m_out[...] = ins[1][...]
            acc_out[...] = ins[2][...]
        else:
            off_out[...] = jnp.zeros((8, 128), F32)
            m_out[...] = jnp.full(m_out.shape, NEG, F32)
            acc_out[...] = jnp.zeros(acc_out.shape, F32)


def last_kernel(
    ids_ref, qa_ref, kv0_ref, kv1_ref, foff, fm, facc, boff, bm, bacc, out_ref,
    off_s, m_s, acc_s, ka_ref, vt_ref,
):
    valid = ids_ref[0] >= 4
    blocks = [(kv0_ref, 0), (kv0_ref, 1), (kv1_ref, 0), (kv1_ref, 1)]

    @pl.when(valid)
    def _():
        offsets, total = slab_offsets(blocks)
        base = foff[:1, :] - total
        fill(blocks, shifted(offsets, base), ka_ref, vt_ref)
        attend(qa_ref, ka_ref, vt_ref, None, (fm, facc), (m_s, acc_s))
        off_s[...] = jnp.broadcast_to(base, (8, 128))

    @pl.when(jnp.logical_not(valid))
    def _():
        off_s[...] = foff[...]
        m_s[...] = fm[...]
        acc_s[...] = facc[...]

    shift = (boff[:1, :] - off_s[:1, :])[:, :1]
    stats = []
    for i in range(TILES):
        best_f = m_s[i, :1, :]
        best_b = jnp.where(bacc[i, 128:129, :] > 0.0, bm[i, :1, :] + shift, NEG)
        best = jnp.maximum(best_f, best_b)
        safe = jnp.where(best < -1e29, 0.0, best)
        wf = jnp.exp(best_f - safe)
        wb = jnp.exp(best_b - safe)
        total = wf * acc_s[i, 128:129, :] + wb * bacc[i, 128:129, :]
        some = total > 0.0
        total = jnp.where(some, total, 1.0)
        wf = wf / total
        wb = wb / total
        mix = wf * acc_s[i, :128, :] + wb * bacc[i, :128, :]
        lse = jnp.where(some, best + jnp.log(total), NEG)
        for g in range(QT // 128):
            row = i * QT % BLOCK + g * 128
            tile = mix[:, g * 128 : (g + 1) * 128].T
            out_ref[i * QT // BLOCK, row : row + 128, :] = tile.astype(BF)
            stats.append(lse[:, g * 128 : (g + 1) * 128])
    for i in range(NX):
        part = jnp.concatenate(stats[4 * i : 4 * i + 4], axis=0)
        rows = jnp.concatenate([*thirds(part), jnp.zeros((META - 12, 128), F32)], axis=0)
        out_ref[i, BLOCK:, :] = rows.astype(BF)


def join_kernel(part_ref, gate_ref, out_ref):
    for a in range(2):
        lses = []
        for b in range(2):
            meta = part_ref[2 * b + a, BLOCK:, :].astype(F32)
            lses.append(meta[0:4] + meta[4:8] + meta[8:12])
        share = 1.0 / (1.0 + jnp.exp(lses[1] - lses[0]))
        for g in range(4):
            rows = slice(g * 128, (g + 1) * 128)
            w0 = jnp.broadcast_to(share[g : g + 1], (128, 128)).T
            p0 = part_ref[a, rows, :].astype(F32)
            p1 = part_ref[2 + a, rows, :].astype(F32)
            att = ((w0 * p0 + (1.0 - w0) * p1) * gate_ref[a, rows, :]).astype(BF)
            for h in range(2):
                out_ref[2 * g + h, :, a * 128 : (a + 1) * 128] = att[h * PIECE : (h + 1) * PIECE]


def out_kernel(rows_ref, wo_ref, out_ref, lhs_ref):
    for j in range(NY * NC):
        lhs_ref[:, j * COLS : (j + 1) * COLS] = rows_ref[j]
    out_ref[...] = jnp.dot(lhs_ref[...], wo_ref[...], preferred_element_type=F32).astype(BF)


def shape(*dims, dtype=BF):
    return jax.ShapeDtypeStruct(dims, dtype)


def call(kernel, outs, specs, flops, scratch=(), alias=None, mib=16, exps=0):
    return pl.pallas_call(
        kernel,
        out_shape=outs,
        in_specs=specs,
        out_specs=jax.tree.map(lambda _: vspec(), outs),
        scratch_shapes=scratch,
        input_output_aliases=alias or {},
        cost_estimate=pl.CostEstimate(
            flops=flops, bytes_accessed=2 << 20, transcendentals=exps
        ),
        compiler_params=pltpu.CompilerParams(vmem_limit_bytes=mib << 20),
    )


STATE = (
    shape(8, 128, dtype=F32),
    shape(TILES, 8, QT, dtype=F32),
    shape(TILES, ACC, QT, dtype=F32),
)
LOADED = [VMEM((KEYS, 256), BF), VMEM((ACC, KEYS), BF)]


def attention(kernel, outs, n_in, alias=None, scratch=()):
    specs = [sspec()] + [vspec()] * (n_in - 1)
    flops = 4 * SLAB * KEYS * 128
    return call(kernel, outs, specs, flops, [*scratch, *LOADED], alias, 28, SLAB * KEYS)


def ring(size, step):
    return [(i, (i + step) % size) for i in range(size)]


def body(tokens, wq, wk, wv, wg, fw, fbias, wo):
    ids = jnp.stack([lax.axis_index(a) for a in AXES]).astype(jnp.int32)

    near = [tokens] + [lax.ppermute(tokens, "y", ring(NY, s)) for s in (1, 2, 3)]
    far = [lax.ppermute(t, "c", ring(NC, 1)) for t in near]
    flops = 2 * BLOCK * WIDTH * COLS
    hbm = pl.BlockSpec(memory_space=pltpu.HBM)
    room = [
        VMEM((BLOCK, WIDTH), BF),
        VMEM((WIDTH, COLS), BF),
        VMEM((WIDTH, COLS), BF),
        pltpu.SemaphoreType.DMA((16,)),
    ]
    kvx = call(
        kv_kernel,
        shape(NX, ROWS, 128),
        [sspec()] + [hbm] * 10 + [vspec(), sspec()],
        2 * flops,
        [*room, VMEM((3, 16, BLOCK), F32)],
        mib=60,
    )(ids, *near, *far, wk, wv, fw.T, fbias)
    kv = lax.all_to_all(kvx, "x", 0, 0, tiled=True)
    qx, gate = call(
        query_kernel,
        (shape(NX, BLOCK, 128), shape(2, BLOCK, 128, dtype=F32)),
        [sspec()] + [hbm] * 10,
        2 * flops,
        room,
        mib=60,
    )(ids, *near, *far, wq, wg)
    q = lax.all_to_all(qx, "x", 0, 0, tiled=True).reshape(SLAB, 128)

    def hop(value, direction):
        return lax.ppermute(value, "z", ring(NZ, direction))

    kf, kb = [kv], [kv]
    for _ in range(1, 4):
        kf.append(hop(kf[-1], 1))
        kb.append(hop(kb[-1], -1))
    far0 = hop(kf[3][:2], 1)
    far1 = hop(kb[3][2:], -1)

    ids = pl.pallas_call(
        arrived_kernel,
        out_shape=shape(4, dtype=jnp.int32),
        in_specs=[sspec(), hbm, hbm],
        out_specs=sspec(),
        name="arrived",
    )(ids, kf[1], kb[1])
    qa, *front = attention(diag_kernel, (shape(SLAB, 256), *STATE), 3)(ids, q, kv)
    back = []
    for s in range(1, 4):
        back = attention(
            functools.partial(back_kernel, s), STATE, 3 + len(back),
            {3: 0, 4: 1, 5: 2} if back else None,
        )(ids, qa, kb[s], *back)
        front = attention(
            functools.partial(front_kernel, s), STATE, 6, {3: 0, 4: 1, 5: 2}
        )(ids, qa, kf[s], *front)
    outs = attention(
        last_kernel, shape(NX, BLOCK + META, 128), 10, None, [VMEM(s.shape, F32) for s in STATE]
    )(ids, qa, far0, far1, *front, *back)
    parts = lax.all_to_all(outs, "x", 0, 0, tiled=True)
    att = call(join_kernel, shape(NY * NC, PIECE, COLS), [vspec()] * 2, 1 << 20)(parts, gate)
    rows = lax.all_to_all(att, ("y", "c"), 0, 0, tiled=True)
    return call(
        out_kernel, shape(PIECE, WIDTH), [vspec()] * 2, 2 * PIECE * WIDTH * WIDTH,
        [VMEM((PIECE, WIDTH), BF)],
    )(rows, wo)


AXES = ("z", "x", "y", "c")


def solution(mesh):
    grid = Mesh(mesh.devices.reshape(NZ, NX, NY, NC), AXES)
    cols = P(None, ("y", "c"))

    return jax.shard_map(
        body,
        mesh=grid,
        in_specs=(P(AXES, None), cols, cols, cols, cols, P(), P(), P()),
        out_specs=P(AXES, None),
        check_vma=False,
    )
```

profile of v0, /device:TPU:224, one launch (start us, length us, event | category | flops | bytes accessed | tf_op | source)
XLA Modules:
  0.0 132.6 jit_solution(8315999014979059949)
XLA Ops:
  0.0 1.6 %collective-permute-start = (bf16[64,2048]{1,0:T(8,128)(2,1)}, bf16[64,2048]{1,0:T(8,128)(2,1)S(1)}, u32[]{:S(2)}, u32[]{:S(2)}) collective-permute-start(bf16[64,2048]{1,0:T(8,128)(2,1)} %refs_0_.3), channel_id=1, source_target_pairs={{0,2},{2,4},{4,6},{6,0},{1,3},{3,5},{5,7},{7,1},{8,10},{10,12},{12... | collective-permute-start | bytes 786440 | tf_op jit(solution)/shard_map/ppermute | solution.py:385
  1.6 2.9 %collective-permute-start.1 = (bf16[64,2048]{1,0:T(8,128)(2,1)}, bf16[64,2048]{1,0:T(8,128)(2,1)S(1)}, u32[]{:S(2)}, u32[]{:S(2)}) collective-permute-start(bf16[64,2048]{1,0:T(8,128)(2,1)} %refs_0_.3), channel_id=1, source_target_pairs={{0,4},{2,6},{4,0},{6,2},{1,5},{3,7},{5,1},{7,3},{8,12},{10,14},{12... | collective-permute-start | bytes 786440 | tf_op jit(solution)/shard_map/ppermute | solution.py:385
  4.5 1.3 %collective-permute-start.2 = (bf16[64,2048]{1,0:T(8,128)(2,1)}, bf16[64,2048]{1,0:T(8,128)(2,1)S(1)}, u32[]{:S(2)}, u32[]{:S(2)}) collective-permute-start(bf16[64,2048]{1,0:T(8,128)(2,1)} %refs_0_.3), channel_id=1, source_target_pairs={{0,6},{2,0},{4,2},{6,4},{1,7},{3,1},{5,3},{7,5},{8,14},{10,8},{12,... | collective-permute-start | bytes 786440 | tf_op jit(solution)/shard_map/ppermute | solution.py:385
  5.8 3.7 %collective-permute-done.refs_1_ = bf16[64,2048]{1,0:T(8,128)(2,1)S(1)} collective-permute-done((bf16[64,2048]{1,0:T(8,128)(2,1)}, bf16[64,2048]{1,0:T(8,128)(2,1)S(1)}, u32[]{:S(2)}, u32[]{:S(2)}) %collective-permute-start) | collective-permute-done | bytes 262176 | tf_op jit(solution)/shard_map/ppermute | solution.py:385
  9.5 6.8 %collective-permute-done.1.refs_2_ = bf16[64,2048]{1,0:T(8,128)(2,1)S(1)} collective-permute-done((bf16[64,2048]{1,0:T(8,128)(2,1)}, bf16[64,2048]{1,0:T(8,128)(2,1)S(1)}, u32[]{:S(2)}, u32[]{:S(2)}) %collective-permute-start.1) | collective-permute-done | bytes 262176 | tf_op jit(solution)/shard_map/ppermute | solution.py:385
  16.3 0.5 collective-permute-start.6
  16.8 0.6 pad_add_fusion.ids_ref
  18.9 6.0 %shard_map.82 = bf16[4,528,128]{2,1,0:T(8,128)(2,1)} custom-call(s32[4]{0:T(128)} %pad_add_fusion.ids_ref, bf16[64,2048]{1,0:T(8,128)(2,1)} %refs_0_.3, bf16[64,2048]{1,0:T(8,128)(2,1)} %copy-done.6, bf16[64,2048]{1,0:T(8,128)(2,1)} %copy-done.7, bf16[64,2048]{1,0:T(8,128)(2,1)} %copy-done.8, bf16[64,2048]{1,0:T(8,128)(2,1)} %copy-done.9, ...), custom_call_target="tpu_custom_call" | custom-call | flops 1073741824 | bytes 2097152 | tf_op jit(solution)/shard_map/pallas_call | solution.py:395
  24.9 14.3 %all_to_all.20.kv_ref = bf16[4,528,128]{2,1,0:T(8,128)(2,1)S(1)} all-to-all(bf16[4,528,128]{2,1,0:T(8,128)(2,1)} %shard_map.82), channel_id=1, replica_groups=mesh['z'=8,'x'=4,'y'=4,'c'=2] {'x'}, dimensions={0} | all-to-all | bytes 1081344 | tf_op jit(solution)/shard_map/all_to_all | solution.py:403
  39.2 2.0 %collective-permute-start.8 = (bf16[4,528,128]{2,1,0:T(8,128)(2,1)S(1)}, bf16[4,528,128]{2,1,0:T(8,128)(2,1)S(1)}, u32[]{:S(2)}, u32[]{:S(2)}) collective-permute-start(bf16[4,528,128]{2,1,0:T(8,128)(2,1)S(1)} %all_to_all.20.kv_ref), channel_id=1, source_target_pairs={{0,224},{32,0},{64,32},{96,64},{128,96},{160,128},{192,160},{224,1... | collective-permute-start | bytes 1622024 | tf_op jit(solution)/shard_map/ppermute | solution.py:415
  41.2 11.2 %collective-permute-done.7.front_ref.kv_ref = bf16[4,528,128]{2,1,0:T(8,128)(2,1)S(1)} collective-permute-done((bf16[4,528,128]{2,1,0:T(8,128)(2,1)S(1)}, bf16[4,528,128]{2,1,0:T(8,128)(2,1)S(1)}, u32[]{:S(2)}, u32[]{:S(2)}) %collective-permute-start.7) | collective-permute-done | bytes 540704 | tf_op jit(solution)/shard_map/ppermute | solution.py:415
  52.4 1.5 %collective-permute-start.9 = (bf16[4,528,128]{2,1,0:T(8,128)(2,1)S(1)}, bf16[4,528,128]{2,1,0:T(8,128)(2,1)S(1)}, u32[]{:S(2)}, u32[]{:S(2)}) collective-permute-start(bf16[4,528,128]{2,1,0:T(8,128)(2,1)S(1)} %collective-permute-done.7.front_ref.kv_ref), channel_id=1, source_target_pairs={{0,32},{32,64},{64,96},{96,128},{128,160},{160,192},{192,224},{224... | collective-permute-start | bytes 1622024 | tf_op jit(solution)/shard_map/ppermute | solution.py:415
  53.9 0.5 collective-permute-start.12
  54.4 5.2 %shard_map.83 = (bf16[4,512,128]{2,1,0:T(8,128)(2,1)}, f32[2,512,128]{2,1,0:T(8,128)}) custom-call(s32[4]{0:T(128)} %pad_add_fusion.ids_ref, bf16[64,2048]{1,0:T(8,128)(2,1)} %refs_0_.3, bf16[64,2048]{1,0:T(8,128)(2,1)} %copy-done.6, bf16[64,2048]{1,0:T(8,128)(2,1)} %copy-done.7, bf16[64,2048]{1,0:T(8,128)(2,1)} %copy-done.8, bf16[64,2048]{1,0:T(8,128)(2,1)} %copy-done.9, ...), custom_call_target="tpu_custom_call" | custom-call | flops 1073741824 | bytes 2097152 | tf_op jit(solution)/shard_map/pallas_call | solution.py:404
  59.6 3.5 %all-to-all-start.1 = ((bf16[4,512,128]{2,1,0:T(8,128)(2,1)}), bf16[4,512,128]{2,1,0:T(8,128)(2,1)S(1)}, u32[]{:S(2)}, u32[]{:S(2)}) async-start(bf16[4,512,128]{2,1,0:T(8,128)(2,1)} %get-tuple-element.29), calls=%async_computation.1 | async-start | bytes 1048576 | tf_op jit(solution)/shard_map/all_to_all | solution.py:412
  63.1 1.7 %collective-permute-done.9.kv_ref = bf16[4,528,128]{2,1,0:T(8,128)(2,1)S(1)} collective-permute-done((bf16[4,528,128]{2,1,0:T(8,128)(2,1)S(1)}, bf16[4,528,128]{2,1,0:T(8,128)(2,1)S(1)}, u32[]{:S(2)}, u32[]{:S(2)}) %collective-permute-start.9) | collective-permute-done | bytes 540704 | tf_op jit(solution)/shard_map/ppermute | solution.py:415
  64.8 2.9 %collective-permute-start.10 = (bf16[4,528,128]{2,1,0:T(8,128)(2,1)S(1)}, bf16[4,528,128]{2,1,0:T(8,128)(2,1)S(1)}, u32[]{:S(2)}, u32[]{:S(2)}) collective-permute-start(bf16[4,528,128]{2,1,0:T(8,128)(2,1)S(1)} %collective-permute-done.9.kv_ref), channel_id=1, source_target_pairs={{0,32},{32,64},{64,96},{96,128},{128,160},{160,192},{192,224},{224... | collective-permute-start | bytes 1622024 | tf_op jit(solution)/shard_map/ppermute | solution.py:415
  67.7 1.2 arrived.1.ids_ref
  68.9 2.2 %all-to-all-done.1 = bf16[4,512,128]{2,1,0:T(8,128)(2,1)S(1)} async-done(((bf16[4,512,128]{2,1,0:T(8,128)(2,1)}), bf16[4,512,128]{2,1,0:T(8,128)(2,1)S(1)}, u32[]{:S(2)}, u32[]{:S(2)}) %all-to-all-start.1) | async-done | bytes 524320 | tf_op jit(solution)/shard_map/all_to_all | solution.py:412
  71.2 0.7 copy-done.5
  71.8 3.2 %shard_map.84 = (bf16[2048,256]{1,0:T(8,128)(2,1)S(1)}, f32[8,128]{1,0:T(8,128)S(1)}, f32[8,8,256]{2,1,0:T(8,128)S(1)}, f32[8,144,256]{2,1,0:T(8,128)S(1)}) custom-call(s32[4]{0:T(128)S(1)} %copy-done.5, bf16[2048,128]{1,0:T(8,128)(2,1)S(1)} %bitcast.8, bf16[4,528,128]{2,1,0:T(8,128)(2,1)S(1)} %all_to_all.20.kv_ref), custom_call_target="tpu_custom_call" | custom-call | flops 1073741824 | bytes 2097152 | tf_op jit(solution)/shard_map/pallas_call | solution.py:431
  75.0 4.3 %shard_map.88 = (f32[8,128]{1,0:T(8,128)S(1)}, f32[8,8,256]{2,1,0:T(8,128)S(1)}, f32[8,144,256]{2,1,0:T(8,128)S(1)}) custom-call(s32[4]{0:T(128)S(1)} %copy-done.5, bf16[2048,256]{1,0:T(8,128)(2,1)S(1)} %get-tuple-element.30.qa_ref, bf16[4,528,128]{2,1,0:T(8,128)(2,1)S(1)} %copy-done.3), custom_call_target="tpu_custom_call" | custom-call | flops 1073741824 | bytes 2097152 | tf_op jit(solution)/shard_map/pallas_call | solution.py:434
  79.3 4.4 %shard_map.85 = (f32[8,128]{1,0:T(8,128)S(1)}, f32[8,8,256]{2,1,0:T(8,128)S(1)}, f32[8,144,256]{2,1,0:T(8,128)S(1)}) custom-call(s32[4]{0:T(128)S(1)} %copy-done.5, bf16[2048,256]{1,0:T(8,128)(2,1)S(1)} %get-tuple-element.30.qa_ref, bf16[4,528,128]{2,1,0:T(8,128)(2,1)S(1)} %copy-done.1, ...), custom_call_target="tpu_custom_call", output_to_operand_aliasing={{0}: (3, {}), {1}: (4, {}), {2}: (5, {})} | custom-call | flops 1073741824 | bytes 2097152 | tf_op jit(solution)/shard_map/pallas_call | solution.py:438
  83.7 4.4 %shard_map.89 = (f32[8,128]{1,0:T(8,128)S(1)}, f32[8,8,256]{2,1,0:T(8,128)S(1)}, f32[8,144,256]{2,1,0:T(8,128)S(1)}) custom-call(s32[4]{0:T(128)S(1)} %copy-done.5, bf16[2048,256]{1,0:T(8,128)(2,1)S(1)} %get-tuple-element.30.qa_ref, ...), custom_call_target="tpu_custom_call", output_to_operand_aliasing={{0}: (3, {}), {1}: (4, {}), {2}: (5, {})} | custom-call | flops 1073741824 | bytes 2097152 | tf_op jit(solution)/shard_map/pallas_call | solution.py:434
  88.3 2.1 %collective-permute-start.14 = (bf16[2,528,128]{2,1,0:T(8,128)(2,1)S(1)}, bf16[2,528,128]{2,1,0:T(8,128)(2,1)S(1)}, u32[]{:S(2)}, u32[]{:S(2)}) collective-permute-start(bf16[2,528,128]{2,1,0:T(8,128)(2,1)S(1)} %slice.9), channel_id=1, source_target_pairs={{0,224},{32,0},{64,32},{96,64},{128,96},{160,128},{192,160},{224,1... | collective-permute-start | bytes 811016 | tf_op jit(solution)/shard_map/ppermute | solution.py:415
  90.4 4.4 %shard_map.86 = (f32[8,128]{1,0:T(8,128)S(1)}, f32[8,8,256]{2,1,0:T(8,128)S(1)}, f32[8,144,256]{2,1,0:T(8,128)S(1)}) custom-call(s32[4]{0:T(128)S(1)} %copy-done.5, bf16[2048,256]{1,0:T(8,128)(2,1)S(1)} %get-tuple-element.30.qa_ref, ...), custom_call_target="tpu_custom_call", output_to_operand_aliasing={{0}: (3, {}), {1}: (4, {}), {2}: (5, {})} | custom-call | flops 1073741824 | bytes 2097152 | tf_op jit(solution)/shard_map/pallas_call | solution.py:438
  94.8 4.6 %shard_map.90 = (f32[8,128]{1,0:T(8,128)S(1)}, f32[8,8,256]{2,1,0:T(8,128)S(1)}, f32[8,144,256]{2,1,0:T(8,128)S(1)}) custom-call(s32[4]{0:T(128)S(1)} %copy-done.5, bf16[2048,256]{1,0:T(8,128)(2,1)S(1)} %get-tuple-element.30.qa_ref, ...), custom_call_target="tpu_custom_call", output_to_operand_aliasing={{0}: (3, {}), {1}: (4, {}), {2}: (5, {})} | custom-call | flops 1073741824 | bytes 2097152 | tf_op jit(solution)/shard_map/pallas_call | solution.py:434
  99.5 4.4 %shard_map.87 = (f32[8,128]{1,0:T(8,128)S(1)}, f32[8,8,256]{2,1,0:T(8,128)S(1)}, f32[8,144,256]{2,1,0:T(8,128)S(1)}) custom-call(s32[4]{0:T(128)S(1)} %copy-done.5, bf16[2048,256]{1,0:T(8,128)(2,1)S(1)} %get-tuple-element.30.qa_ref, ...), custom_call_target="tpu_custom_call", output_to_operand_aliasing={{0}: (3, {}), {1}: (4, {}), {2}: (5, {})} | custom-call | flops 1073741824 | bytes 2097152 | tf_op jit(solution)/shard_map/pallas_call | solution.py:438
  103.9 4.8 %shard_map.91 = bf16[4,528,128]{2,1,0:T(8,128)(2,1)S(1)} custom-call(s32[4]{0:T(128)S(1)} %copy-done.5, bf16[2048,256]{1,0:T(8,128)(2,1)S(1)} %get-tuple-element.30.qa_ref, bf16[2,528,128]{2,1,0:T(8,128)(2,1)S(1)} %collective-permute-done.11.kv0_ref, bf16[2,528,128]{2,1,0:T(8,128)(2,1)S(1)} %collective-permute-done.14.kv1_ref, ...), custom_call_target="tpu_custom_call" | custom-call | flops 1073741824 | bytes 2097152 | tf_op jit(solution)/shard_map/pallas_call | solution.py:441
  108.7 10.7 %all_to_all.21.part_ref = bf16[4,528,128]{2,1,0:T(8,128)(2,1)S(1)} all-to-all(bf16[4,528,128]{2,1,0:T(8,128)(2,1)S(1)} %shard_map.91), channel_id=1, replica_groups=mesh['z'=8,'x'=4,'y'=4,'c'=2] {'x'}, dimensions={0} | all-to-all | bytes 1081344 | tf_op jit(solution)/shard_map/all_to_all | solution.py:444
  119.6 10.8 %all_to_all.22.rows_ref = bf16[8,64,256]{2,1,0:T(8,128)(2,1)S(1)} all-to-all(bf16[8,64,256]{2,1,0:T(8,128)(2,1)S(1)} %shard_map.92), channel_id=1, replica_groups=mesh['z'=8,'x'=4,'y'=4,'c'=2] {'y','c'}, dimensions={0} | all-to-all | bytes 524288 | tf_op jit(solution)/shard_map/all_to_all | solution.py:446
  130.4 2.3 %shard_map.93 = bf16[64,2048]{1,0:T(8,128)(2,1)} custom-call(bf16[8,64,256]{2,1,0:T(8,128)(2,1)S(1)} %all_to_all.22.rows_ref, bf16[2048,2048]{1,0:T(8,128)(2,1)S(1)} %bitcast.7), custom_call_target="tpu_custom_call" | custom-call | flops 536870912 | bytes 2097152 | tf_op jit(solution)/shard_map/pallas_call | solution.py:447
  (50 shorter events, 1.9 us)
Async XLA Ops:
  0.0 9.5 %collective-permute-start = (bf16[64,2048]{1,0:T(8,128)(2,1)}, bf16[64,2048]{1,0:T(8,128)(2,1)S(1)}, u32[]{:S(2)}, u32[]{:S(2)}) collective-permute-start(bf16[64,2048]{1,0:T(8,128)(2,1)} %refs_0_.3), channel_id=1, source_target_pairs={{0,2},{2,4},{4,6},{6,0},{1,3},{3,5},{5,7},{7,1},{8,10},{10,12},{12... | collective-permute-start | bytes 786440 | tf_op jit(solution)/shard_map/ppermute | solution.py:385
  1.6 14.7 %collective-permute-start.1 = (bf16[64,2048]{1,0:T(8,128)(2,1)}, bf16[64,2048]{1,0:T(8,128)(2,1)S(1)}, u32[]{:S(2)}, u32[]{:S(2)}) collective-permute-start(bf16[64,2048]{1,0:T(8,128)(2,1)} %refs_0_.3), channel_id=1, source_target_pairs={{0,4},{2,6},{4,0},{6,2},{1,5},{3,7},{5,1},{7,3},{8,12},{10,14},{12... | collective-permute-start | bytes 786440 | tf_op jit(solution)/shard_map/ppermute | solution.py:385
  4.5 11.9 %collective-permute-start.2 = (bf16[64,2048]{1,0:T(8,128)(2,1)}, bf16[64,2048]{1,0:T(8,128)(2,1)S(1)}, u32[]{:S(2)}, u32[]{:S(2)}) collective-permute-start(bf16[64,2048]{1,0:T(8,128)(2,1)} %refs_0_.3), channel_id=1, source_target_pairs={{0,6},{2,0},{4,2},{6,4},{1,7},{3,1},{5,3},{7,5},{8,14},{10,8},{12,... | collective-permute-start | bytes 786440 | tf_op jit(solution)/shard_map/ppermute | solution.py:385
  5.8 11.6 %collective-permute-start.3 = (bf16[64,2048]{1,0:T(8,128)(2,1)}, bf16[64,2048]{1,0:T(8,128)(2,1)S(1)}, u32[]{:S(2)}, u32[]{:S(2)}) collective-permute-start(bf16[64,2048]{1,0:T(8,128)(2,1)} %refs_0_.3), channel_id=1, source_target_pairs={{0,1},{1,0},{2,3},{3,2},{4,5},{5,4},{6,7},{7,6},{8,9},{9,8},{10,11... | collective-permute-start | bytes 786440 | tf_op jit(solution)/shard_map/ppermute | solution.py:386
  9.5 8.7 %copy-start.6 = (bf16[64,2048]{1,0:T(8,128)(2,1)}, bf16[64,2048]{1,0:T(8,128)(2,1)S(1)}, u32[]{:S(2)}) copy-start(bf16[64,2048]{1,0:T(8,128)(2,1)S(1)} %collective-permute-done.refs_1_) | copy-start | bytes 786436
  9.5 7.9 %collective-permute-start.4 = (bf16[64,2048]{1,0:T(8,128)(2,1)S(1)}, bf16[64,2048]{1,0:T(8,128)(2,1)S(1)}, u32[]{:S(2)}, u32[]{:S(2)}) collective-permute-start(bf16[64,2048]{1,0:T(8,128)(2,1)S(1)} %collective-permute-done.refs_1_), channel_id=1, source_target_pairs={{0,1},{1,0},{2,3},{3,2},{4,5},{5,4},{6,7},{7,6},{8,9},{9,8},{10,11... | collective-permute-start | bytes 786440 | tf_op jit(solution)/shard_map/ppermute | solution.py:386
  16.3 1.9 %copy-start.7 = (bf16[64,2048]{1,0:T(8,128)(2,1)}, bf16[64,2048]{1,0:T(8,128)(2,1)S(1)}, u32[]{:S(2)}) copy-start(bf16[64,2048]{1,0:T(8,128)(2,1)S(1)} %collective-permute-done.1.refs_2_) | copy-start | bytes 786436
  16.3 1.5 %collective-permute-start.5 = (bf16[64,2048]{1,0:T(8,128)(2,1)S(1)}, bf16[64,2048]{1,0:T(8,128)(2,1)S(1)}, u32[]{:S(2)}, u32[]{:S(2)}) collective-permute-start(bf16[64,2048]{1,0:T(8,128)(2,1)S(1)} %collective-permute-done.1.refs_2_), channel_id=1, source_target_pairs={{0,1},{1,0},{2,3},{3,2},{4,5},{5,4},{6,7},{7,6},{8,9},{9,8},{10,11... | collective-permute-start | bytes 786440 | tf_op jit(solution)/shard_map/ppermute | solution.py:386
  16.3 1.9 %copy-start.8 = (bf16[64,2048]{1,0:T(8,128)(2,1)}, bf16[64,2048]{1,0:T(8,128)(2,1)S(1)}, u32[]{:S(2)}) copy-start(bf16[64,2048]{1,0:T(8,128)(2,1)S(1)} %collective-permute-done.2.refs_3_) | copy-start | bytes 786436
  16.3 1.9 %collective-permute-start.6 = (bf16[64,2048]{1,0:T(8,128)(2,1)S(1)}, bf16[64,2048]{1,0:T(8,128)(2,1)S(1)}, u32[]{:S(2)}, u32[]{:S(2)}) collective-permute-start(bf16[64,2048]{1,0:T(8,128)(2,1)S(1)} %collective-permute-done.2.refs_3_), channel_id=1, source_target_pairs={{0,1},{1,0},{2,3},{3,2},{4,5},{5,4},{6,7},{7,6},{8,9},{9,8},{10,11... | collective-permute-start | bytes 786440 | tf_op jit(solution)/shard_map/ppermute | solution.py:386
  17.4 0.8 copy-start.9
  17.5 0.8 copy-start.10
  17.9 0.7 copy-start.11
  18.2 0.7 copy-start.12
  39.2 13.2 %collective-permute-start.7 = (bf16[4,528,128]{2,1,0:T(8,128)(2,1)S(1)}, bf16[4,528,128]{2,1,0:T(8,128)(2,1)S(1)}, u32[]{:S(2)}, u32[]{:S(2)}) collective-permute-start(bf16[4,528,128]{2,1,0:T(8,128)(2,1)S(1)} %all_to_all.20.kv_ref), channel_id=1, source_target_pairs={{0,32},{32,64},{64,96},{96,128},{128,160},{160,192},{192,224},{224... | collective-permute-start | bytes 1622024 | tf_op jit(solution)/shard_map/ppermute | solution.py:415
  39.2 14.7 %collective-permute-start.8 = (bf16[4,528,128]{2,1,0:T(8,128)(2,1)S(1)}, bf16[4,528,128]{2,1,0:T(8,128)(2,1)S(1)}, u32[]{:S(2)}, u32[]{:S(2)}) collective-permute-start(bf16[4,528,128]{2,1,0:T(8,128)(2,1)S(1)} %all_to_all.20.kv_ref), channel_id=1, source_target_pairs={{0,224},{32,0},{64,32},{96,64},{128,96},{160,128},{192,160},{224,1... | collective-permute-start | bytes 1622024 | tf_op jit(solution)/shard_map/ppermute | solution.py:415
  52.4 7.2 %copy-start = (bf16[4,528,128]{2,1,0:T(8,128)(2,1)}, bf16[4,528,128]{2,1,0:T(8,128)(2,1)S(1)}, u32[]{:S(2)}) copy-start(bf16[4,528,128]{2,1,0:T(8,128)(2,1)S(1)} %collective-permute-done.7.front_ref.kv_ref) | copy-start | bytes 1622020
  52.4 12.4 %collective-permute-start.9 = (bf16[4,528,128]{2,1,0:T(8,128)(2,1)S(1)}, bf16[4,528,128]{2,1,0:T(8,128)(2,1)S(1)}, u32[]{:S(2)}, u32[]{:S(2)}) collective-permute-start(bf16[4,528,128]{2,1,0:T(8,128)(2,1)S(1)} %collective-permute-done.7.front_ref.kv_ref), channel_id=1, source_target_pairs={{0,32},{32,64},{64,96},{96,128},{128,160},{160,192},{192,224},{224... | collective-permute-start | bytes 1622024 | tf_op jit(solution)/shard_map/ppermute | solution.py:415
  53.9 5.7 %copy-start.2 = (bf16[4,528,128]{2,1,0:T(8,128)(2,1)}, bf16[4,528,128]{2,1,0:T(8,128)(2,1)S(1)}, u32[]{:S(2)}) copy-start(bf16[4,528,128]{2,1,0:T(8,128)(2,1)S(1)} %collective-permute-done.8.back_ref.kv_ref) | copy-start | bytes 1622020
  53.9 13.8 %collective-permute-start.12 = (bf16[4,528,128]{2,1,0:T(8,128)(2,1)S(1)}, bf16[4,528,128]{2,1,0:T(8,128)(2,1)S(1)}, u32[]{:S(2)}, u32[]{:S(2)}) collective-permute-start(bf16[4,528,128]{2,1,0:T(8,128)(2,1)S(1)} %collective-permute-done.8.back_ref.kv_ref), channel_id=1, source_target_pairs={{0,224},{32,0},{64,32},{96,64},{128,96},{160,128},{192,160},{224,1... | collective-permute-start | bytes 1622024 | tf_op jit(solution)/shard_map/ppermute | solution.py:415
  59.6 11.5 %all-to-all-start.1 = ((bf16[4,512,128]{2,1,0:T(8,128)(2,1)}), bf16[4,512,128]{2,1,0:T(8,128)(2,1)S(1)}, u32[]{:S(2)}, u32[]{:S(2)}) async-start(bf16[4,512,128]{2,1,0:T(8,128)(2,1)} %get-tuple-element.29), calls=%async_computation.1 | async-start | bytes 1048576 | tf_op jit(solution)/shard_map/all_to_all | solution.py:412
  64.8 23.3 %collective-permute-start.10 = (bf16[4,528,128]{2,1,0:T(8,128)(2,1)S(1)}, bf16[4,528,128]{2,1,0:T(8,128)(2,1)S(1)}, u32[]{:S(2)}, u32[]{:S(2)}) collective-permute-start(bf16[4,528,128]{2,1,0:T(8,128)(2,1)S(1)} %collective-permute-done.9.kv_ref), channel_id=1, source_target_pairs={{0,32},{32,64},{64,96},{96,128},{128,160},{160,192},{192,224},{224... | collective-permute-start | bytes 1622024 | tf_op jit(solution)/shard_map/ppermute | solution.py:415
  67.7 20.6 %collective-permute-start.13 = (bf16[4,528,128]{2,1,0:T(8,128)(2,1)S(1)}, bf16[4,528,128]{2,1,0:T(8,128)(2,1)S(1)}, u32[]{:S(2)}, u32[]{:S(2)}) collective-permute-start(bf16[4,528,128]{2,1,0:T(8,128)(2,1)S(1)} %collective-permute-done.12.kv_ref), channel_id=1, source_target_pairs={{0,224},{32,0},{64,32},{96,64},{128,96},{160,128},{192,160},{224,1... | collective-permute-start | bytes 1622024 | tf_op jit(solution)/shard_map/ppermute | solution.py:415
  71.2 0.7 copy-start.5
  71.8 3.2 %copy-start.3 = (bf16[4,528,128]{2,1,0:T(8,128)(2,1)S(1)}, bf16[4,528,128]{2,1,0:T(8,128)(2,1)}, u32[]{:S(2)}) copy-start(bf16[4,528,128]{2,1,0:T(8,128)(2,1)} %copy-done.2) | copy-start | bytes 1622020
  75.0 4.3 %copy-start.1 = (bf16[4,528,128]{2,1,0:T(8,128)(2,1)S(1)}, bf16[4,528,128]{2,1,0:T(8,128)(2,1)}, u32[]{:S(2)}) copy-start(bf16[4,528,128]{2,1,0:T(8,128)(2,1)} %copy-done) | copy-start | bytes 1622020
  88.2 15.7 %collective-permute-start.11 = (bf16[2,528,128]{2,1,0:T(8,128)(2,1)S(1)}, bf16[2,528,128]{2,1,0:T(8,128)(2,1)S(1)}, u32[]{:S(2)}, u32[]{:S(2)}) collective-permute-start(bf16[2,528,128]{2,1,0:T(8,128)(2,1)S(1)} %slice.8), channel_id=1, source_target_pairs={{0,32},{32,64},{64,96},{96,128},{128,160},{160,192},{192,224},{224... | collective-permute-start | bytes 811016 | tf_op jit(solution)/shard_map/ppermute | solution.py:415
  88.3 15.6 %collective-permute-start.14 = (bf16[2,528,128]{2,1,0:T(8,128)(2,1)S(1)}, bf16[2,528,128]{2,1,0:T(8,128)(2,1)S(1)}, u32[]{:S(2)}, u32[]{:S(2)}) collective-permute-start(bf16[2,528,128]{2,1,0:T(8,128)(2,1)S(1)} %slice.9), channel_id=1, source_target_pairs={{0,224},{32,0},{64,32},{96,64},{128,96},{160,128},{192,160},{224,1... | collective-permute-start | bytes 811016 | tf_op jit(solution)/shard_map/ppermute | solution.py:415
  94.8 35.5 %slice-start = ((s8[8388608]{0:T(1024)(128)(4,1)}), s8[4194304]{0:T(1024)(128)(4,1)S(1)}, s32[]{:S(2)}) async-start(s8[8388608]{0:T(1024)(128)(4,1)} %bitcast.6), calls=%async_computation.4 | async-start | bytes 8388608
  99.5 30.9 %slice-start.1 = ((s8[8388608]{0:T(1024)(128)(4,1)}), s8[4194304]{0:T(1024)(128)(4,1)S(1)}, s32[]{:S(2)}) async-start(s8[8388608]{0:T(1024)(128)(4,1)} %bitcast.6), calls=%async_computation.5 | async-start | bytes 8388608
  108.7 10.7 %copy-start.4 = (f32[2,512,128]{2,1,0:T(8,128)S(1)}, f32[2,512,128]{2,1,0:T(8,128)}, u32[]{:S(2)}) copy-start(f32[2,512,128]{2,1,0:T(8,128)} %get-tuple-element.52.gate_ref) | copy-start | bytes 1572868
where the time goes:
time: 133 us
  Pallas kernels  49.3 us (37%)
  blocking collectives  35.7 us (27%)
  waiting for transfers between devices  26.4 us (20%)
  starting transfers between devices  18.9 us (14%)
  local copies, waits for them, and re-layouts  1.41 us (1%)
    all_to_all x1, blocking collectives, body(): kv = lax.all_to_all(kvx, 'x', 0, 0, tiled=True)  14.3 us
    pallas_call x3, Pallas kernels, body(): attention(functools.partial(back_kernel, s), STATE, 3 + len(back), {3: 0,...  13.3 us
    pallas_call x3, Pallas kernels, body(): attention(functools.partial(front_kernel, s), STATE, 6, {3: 0, 4: 1, 5: 2})  13.2 us
    ppermute x8, waiting for transfers between devices, hop(): return lax.ppermute(value, 'z', ring(NZ, direction))  12.9 us
    all_to_all x1, blocking collectives, body(): rows = lax.all_to_all(att, ('y', 'c'), 0, 0, tiled=True)  10.8 us
    all_to_all x1, blocking collectives, body(): parts = lax.all_to_all(outs, 'x', 0, 0, tiled=True)  10.7 us
    ppermute x3, waiting for transfers between devices, body(): lax.ppermute(tokens, 'y', ring(NY, s))  10.5 us
    ppermute x8, starting transfers between devices, hop(): return lax.ppermute(value, 'z', ring(NZ, direction))  9.08 us
  transfers between devices with their start and end apart: 16, of which 7 were waited for; matrix products, arithmetic and copies ran while one was open for 0% of the time, Pallas kernels for 27%

commit v1 on v0

--- a/solution.py
+++ b/solution.py
@@ -43,36 +43,39 @@
     return high, mid, low
 
 
-def gather(ids_ref, pieces, toks_ref, weights, sems):
+def fetch(ids_ref, pieces, toks_ref, weights, sems):
     y, c = ids_ref[2], ids_ref[3]
+    pairs = []
+    for i in range(8):
+        pos = 2 * ((y + NY - i % NY) % NY) + (c if i < NY else 1 - c)
+        start = pl.multiple_of(pos * PIECE, PIECE)
+        pairs.append((pieces[i], toks_ref.at[pl.ds(start, PIECE), :]))
     parts = 4
-    pairs = []
     for source, target in weights:
         for i in range(parts):
             rows = pl.ds(i * WIDTH // parts, WIDTH // parts)
             pairs.append((source.at[rows, :], target.at[rows, :]))
-    for i in range(8):
-        pos = 2 * ((y + NY - i % NY) % NY) + (c if i < NY else 1 - c)
-        start = pl.multiple_of(pos * PIECE, PIECE)
-        pairs.append((pieces[i], toks_ref.at[pl.ds(start, PIECE), :]))
     copies = [
         pltpu.make_async_copy(source, target, sems.at[i])
         for i, (source, target) in enumerate(pairs)
     ]
     for copy in copies:
         copy.start()
+    return copies[:8], copies[8:]
+
+
+def wait_all(copies):
     for copy in copies:
         copy.wait()
-    return toks_ref[...]
 
 
 def kv_kernel(ids_ref, *refs):
     wk_hbm, wv_hbm, fw_ref, bias_ref, kv_ref, toks_ref, wk_ref, wv_ref, sems, parts_ref = refs[8:]
     y, c = ids_ref[2], ids_ref[3]
     weights = [(wk_hbm, wk_ref), (wv_hbm, wv_ref)]
-    toks = gather(ids_ref, refs[:8], toks_ref, weights, sems)
-    keys = jnp.dot(toks, wk_ref[...], preferred_element_type=F32).astype(BF)
-    values = jnp.dot(toks, wv_ref[...], preferred_element_type=F32).astype(BF)
+    toks_copies, weight_copies = fetch(ids_ref, refs[:8], toks_ref, weights, sems)
+    wait_all(toks_copies)
+    toks = toks_ref[...]
     logits = lax.dot_general(
         fw_ref[...], toks, (((1,), (1,)), ((), ())), preferred_element_type=F32
     )
@@ -88,6 +91,9 @@
     )
     for i, part in enumerate(thirds(local)):
         parts_ref[i] = part
+    wait_all(weight_copies)
+    keys = jnp.dot(toks, wk_ref[...], preferred_element_type=F32).astype(BF)
+    values = jnp.dot(toks, wv_ref[...], preferred_element_type=F32)
     for a in range(2):
         head = 2 * (2 * y + c) + a
         mine = [parts_ref[i, pl.ds(head, 1), :] for i in range(3)]
@@ -101,30 +107,34 @@
             rows += [jnp.broadcast_to(part[:, BLOCK - 1 :], (1, 128)) for part in mine]
             rows.append(jnp.zeros((META - 9, 128), F32))
             kv_ref[dest, :HALF, :] = keys[b * HALF : (b + 1) * HALF, a * 128 : (a + 1) * 128]
-            kv_ref[dest, HALF : 2 * HALF, :] = values[
-                b * HALF : (b + 1) * HALF, a * 128 : (a + 1) * 128
-            ]
+            for g in range(2):
+                tile = values[b * HALF + g * 128 : b * HALF + (g + 1) * 128, a * 128 : (a + 1) * 128]
+                kv_ref[dest, HALF + g * 128 : HALF + (g + 1) * 128, :] = tile.T.astype(BF)
             kv_ref[dest, 2 * HALF :, :] = jnp.concatenate(rows, axis=0).astype(BF)
 
 
+def by_parity(ids_ref, both):
+    even = ids_ref[1] % 2 == 0
+    low, high = both[:, :128], both[:, 128:]
+    return jnp.where(even, low, high), jnp.where(even, high, low)
+
+
 def query_kernel(ids_ref, *refs):
-    wq_hbm, wg_hbm, qx_ref, gate_ref, toks_ref, wq_ref, wg_ref, sems = refs[8:]
-    weights = [(wq_hbm, wq_ref), (wg_hbm, wg_ref)]
-    toks = gather(ids_ref, refs[:8], toks_ref, weights, sems)
-    queries = jnp.dot(toks, wq_ref[...], preferred_element_type=F32)
-    queries = (queries * HEAD_DIM**-0.5).astype(BF)
-    for b in range(2):
-        for a in range(2):
-            qx_ref[2 * b + a] = queries[:, a * 128 : (a + 1) * 128]
-    pre = jnp.dot(toks, wg_ref[...], preferred_element_type=F32)
-    gate = 1.0 / (1.0 + jnp.exp(-pre))
-    for a in range(2):
-        gate_ref[a] = gate[:, a * 128 : (a + 1) * 128]
-
-
-def arrived_kernel(ids_ref, front_ref, back_ref, out_ref):
-    for i in range(4):
-        out_ref[i] = ids_ref[i]
+    wq_hbm, same_ref, other_ref, toks_ref, wq_ref, sems = refs[8:]
+    toks_copies, weight_copies = fetch(ids_ref, refs[:8], toks_ref, [(wq_hbm, wq_ref)], sems)
+    wait_all(toks_copies + weight_copies)
+    queries = jnp.dot(toks_ref[...], wq_ref[...], preferred_element_type=F32)
+    same, other = by_parity(ids_ref, queries * HEAD_DIM**-0.5)
+    same_ref[...] = same.astype(BF)
+    other_ref[...] = other.astype(BF)
+
+
+def gate_kernel(ids_ref, *refs):
+    wg_hbm, gate_ref, toks_ref, wg_ref, sems = refs[8:]
+    toks_copies, weight_copies = fetch(ids_ref, refs[:8], toks_ref, [(wg_hbm, wg_ref)], sems)
+    wait_all(toks_copies + weight_copies)
+    pre = jnp.dot(toks_ref[...], wg_ref[...], preferred_element_type=F32)
+    gate_ref[0], gate_ref[1] = by_parity(ids_ref, 1.0 / (1.0 + jnp.exp(-pre)))
 
 
 QT = 256
@@ -134,15 +144,16 @@
 
 
 def fill(blocks, offsets, ka_ref, vt_ref):
-    for j, ((ref, index), (rows, before)) in enumerate(zip(blocks, offsets)):
+    biases = [rows[g] + before for rows, before in offsets for g in range(2)]
+    parts = thirds(-jnp.concatenate(biases, axis=0))
+    turned = jnp.concatenate([*parts, jnp.zeros((104, 128), F32)], axis=0).T
+    lane = lax.broadcasted_iota(jnp.int32, (128, 128), 1)
+    for j, (ref, index) in enumerate(blocks):
         ka_ref[j * HALF : (j + 1) * HALF, :128] = ref[index, :HALF, :]
         for g in range(2):
             cols = slice(j * HALF + g * 128, j * HALF + (g + 1) * 128)
-            parts = thirds(-(rows[g] + before))
-            tile = jnp.concatenate([*parts, jnp.zeros((125, 128), F32)], axis=0)
-            ka_ref[cols, 128:] = tile.T.astype(BF)
-            vals = ref[index, HALF + g * 128 : HALF + (g + 1) * 128, :]
-            vt_ref[:128, cols] = vals.astype(F32).T.astype(BF)
+            ka_ref[cols, 128:] = jnp.where(lane % 8 == 2 * j + g, turned, 0.0).astype(BF)
+            vt_ref[:128, cols] = ref[index, HALF + g * 128 : HALF + (g + 1) * 128, :]
     row = lax.broadcasted_iota(jnp.int32, (ACC - 128, KEYS), 0)
     vt_ref[128:, :] = jnp.where(row == 0, 1.0, 0.0).astype(BF)
 
@@ -212,12 +223,14 @@
     return [(ref, xs) for xs in range(NX)]
 
 
-def diag_kernel(ids_ref, q_ref, kv_ref, qa_out, off_out, m_out, acc_out, ka_ref, vt_ref):
+def diag_kernel(ids_ref, q0, q1, q2, q3, kv_ref, qa_out, off_out, m_out, acc_out, ka_ref, vt_ref):
     offsets, _ = slab_offsets(whole(kv_ref))
     fill(whole(kv_ref), offsets, ka_ref, vt_ref)
     lane = lax.broadcasted_iota(jnp.int32, (SLAB, 128), 1)
-    qa_out[:, :128] = q_ref[...]
-    qa_out[:, 128:] = jnp.where(lane < 3, 1.0, 0.0).astype(BF)
+    for step, q_ref in enumerate((q0, q1, q2, q3)):
+        block = (ids_ref[1] + NX - step) % NX
+        qa_out[pl.ds(pl.multiple_of(block * BLOCK, BLOCK), BLOCK), :128] = q_ref[...]
+    qa_out[:, 128:] = jnp.where(lane < 24, 1.0, 0.0).astype(BF)
     attend(qa_out, ka_ref, vt_ref, ids_ref[1] // 2, None, (m_out, acc_out))
     off_out[...] = jnp.zeros((8, 128), F32)
 
@@ -272,7 +285,7 @@
 
 
 def last_kernel(
-    ids_ref, qa_ref, kv0_ref, kv1_ref, foff, fm, facc, boff, bm, bacc, out_ref,
+    ids_ref, qa_ref, kv0_ref, kv1_ref, foff, fm, facc, boff, bm, bacc, out0, out1, out2, out3,
     off_s, m_s, acc_s, ka_ref, vt_ref,
 ):
     valid = ids_ref[0] >= 4
@@ -293,47 +306,60 @@
         acc_s[...] = facc[...]
 
     shift = (boff[:1, :] - off_s[:1, :])[:, :1]
+    per = BLOCK // QT
+    for step, out_ref in enumerate((out0, out1, out2, out3)):
+        block = (ids_ref[1] + step) % NX
+        stats = []
+        for t in range(per):
+            stats += merge(block * per + t, t, shift, (m_s, acc_s), (bm, bacc), out_ref)
+        part = jnp.concatenate(stats, axis=0)
+        rows = jnp.concatenate([*thirds(part), jnp.zeros((META - 12, 128), F32)], axis=0)
+        out_ref[BLOCK:, :] = rows.astype(BF)
+
+
+def merge(i, t, shift, front, back, out_ref):
+    (m_s, acc_s), (bm, bacc) = front, back
+    best_f = m_s[i, :1, :]
+    best_b = jnp.where(bacc[i, 128:129, :] > 0.0, bm[i, :1, :] + shift, NEG)
+    best = jnp.maximum(best_f, best_b)
+    safe = jnp.where(best < -1e29, 0.0, best)
+    wf = jnp.exp(best_f - safe)
+    wb = jnp.exp(best_b - safe)
+    total = wf * acc_s[i, 128:129, :] + wb * bacc[i, 128:129, :]
+    some = total > 0.0
+    total = jnp.where(some, total, 1.0)
+    wf = wf / total
+    wb = wb / total
+    mix = wf * acc_s[i, :128, :] + wb * bacc[i, :128, :]
+    lse = jnp.where(some, best + jnp.log(total), NEG)
     stats = []
-    for i in range(TILES):
-        best_f = m_s[i, :1, :]
-        best_b = jnp.where(bacc[i, 128:129, :] > 0.0, bm[i, :1, :] + shift, NEG)
-        best = jnp.maximum(best_f, best_b)
-        safe = jnp.where(best < -1e29, 0.0, best)
-        wf = jnp.exp(best_f - safe)
-        wb = jnp.exp(best_b - safe)
-        total = wf * acc_s[i, 128:129, :] + wb * bacc[i, 128:129, :]
-        some = total > 0.0
-        total = jnp.where(some, total, 1.0)
-        wf = wf / total
-        wb = wb / total
-        mix = wf * acc_s[i, :128, :] + wb * bacc[i, :128, :]
-        lse = jnp.where(some, best + jnp.log(total), NEG)
-        for g in range(QT // 128):
-            row = i * QT % BLOCK + g * 128
-            tile = mix[:, g * 128 : (g + 1) * 128].T
-            out_ref[i * QT // BLOCK, row : row + 128, :] = tile.astype(BF)
-            stats.append(lse[:, g * 128 : (g + 1) * 128])
-    for i in range(NX):
-        part = jnp.concatenate(stats[4 * i : 4 * i + 4], axis=0)
-        rows = jnp.concatenate([*thirds(part), jnp.zeros((META - 12, 128), F32)], axis=0)
-        out_ref[i, BLOCK:, :] = rows.astype(BF)
-
-
-def join_kernel(part_ref, gate_ref, out_ref):
-    for a in range(2):
-        lses = []
-        for b in range(2):
-            meta = part_ref[2 * b + a, BLOCK:, :].astype(F32)
-            lses.append(meta[0:4] + meta[4:8] + meta[8:12])
-        share = 1.0 / (1.0 + jnp.exp(lses[1] - lses[0]))
-        for g in range(4):
-            rows = slice(g * 128, (g + 1) * 128)
-            w0 = jnp.broadcast_to(share[g : g + 1], (128, 128)).T
-            p0 = part_ref[a, rows, :].astype(F32)
-            p1 = part_ref[2 + a, rows, :].astype(F32)
-            att = ((w0 * p0 + (1.0 - w0) * p1) * gate_ref[a, rows, :]).astype(BF)
-            for h in range(2):
-                out_ref[2 * g + h, :, a * 128 : (a + 1) * 128] = att[h * PIECE : (h + 1) * PIECE]
+    for g in range(QT // 128):
+        row = t * QT + g * 128
+        out_ref[row : row + 128, :] = mix[:, g * 128 : (g + 1) * 128].T.astype(BF)
+        stats.append(lse[:, g * 128 : (g + 1) * 128])
+    return stats
+
+
+def join_kernel(ids_ref, p0_ref, p1_ref, p2_ref, p3_ref, gate_ref, out_ref):
+    shares = []
+    for one, two in ((p0_ref, p2_ref), (p1_ref, p3_ref)):
+        metas = [ref[BLOCK:, :].astype(F32) for ref in (one, two)]
+        first, second = [meta[0:4] + meta[4:8] + meta[8:12] for meta in metas]
+        shares.append(1.0 / (1.0 + jnp.exp(second - first)))
+    even = ids_ref[1] % 2 == 0
+    for g in range(4):
+        rows = slice(g * 128, (g + 1) * 128)
+        atts = []
+        for a, (one, two) in enumerate(((p0_ref, p2_ref), (p1_ref, p3_ref))):
+            w0 = jnp.broadcast_to(shares[a][g : g + 1], (128, 128)).T
+            mix = w0 * one[rows, :].astype(F32) + (1.0 - w0) * two[rows, :].astype(F32)
+            atts.append(mix * gate_ref[a, rows, :])
+        low = jnp.where(even, atts[0], atts[1]).astype(BF)
+        high = jnp.where(even, atts[1], atts[0]).astype(BF)
+        for h in range(2):
+            part = slice(h * PIECE, (h + 1) * PIECE)
+            out_ref[2 * g + h, :, :128] = low[part]
+            out_ref[2 * g + h, :, 128:] = high[part]
 
 
 def out_kernel(rows_ref, wo_ref, out_ref, lhs_ref):
@@ -383,33 +409,36 @@
     ids = jnp.stack([lax.axis_index(a) for a in AXES]).astype(jnp.int32)
 
     near = [tokens] + [lax.ppermute(tokens, "y", ring(NY, s)) for s in (1, 2, 3)]
-    far = [lax.ppermute(t, "c", ring(NC, 1)) for t in near]
+    far = [lax.ppermute(near[0], "c", ring(NC, 1))]
+    far += [lax.ppermute(t, "c", ring(NC, 1)) for t in near[1:]]
     flops = 2 * BLOCK * WIDTH * COLS
     hbm = pl.BlockSpec(memory_space=pltpu.HBM)
-    room = [
-        VMEM((BLOCK, WIDTH), BF),
-        VMEM((WIDTH, COLS), BF),
-        VMEM((WIDTH, COLS), BF),
-        pltpu.SemaphoreType.DMA((16,)),
-    ]
-    kvx = call(
-        kv_kernel,
-        shape(NX, ROWS, 128),
-        [sspec()] + [hbm] * 10 + [vspec(), sspec()],
-        2 * flops,
-        [*room, VMEM((3, 16, BLOCK), F32)],
-        mib=60,
-    )(ids, *near, *far, wk, wv, fw.T, fbias)
+    weight = VMEM((WIDTH, COLS), BF)
+
+    def project(kernel, outs, weights, extra=(), specs=(), scratch=()):
+        return call(
+            kernel, outs, [sspec()] + [hbm] * (8 + len(weights)) + list(specs),
+            flops * len(weights),
+            [VMEM((BLOCK, WIDTH), BF), *[weight] * len(weights), pltpu.SemaphoreType.DMA((16,))]
+            + list(scratch),
+            mib=60,
+        )(ids, *near, *far, *weights, *extra)
+
+    kvx = project(
+        kv_kernel, shape(NX, ROWS, 128), (wk, wv), (fw.T, fbias),
+        (vspec(), sspec()), (VMEM((3, 16, BLOCK), F32),),
+    )
     kv = lax.all_to_all(kvx, "x", 0, 0, tiled=True)
-    qx, gate = call(
-        query_kernel,
-        (shape(NX, BLOCK, 128), shape(2, BLOCK, 128, dtype=F32)),
-        [sspec()] + [hbm] * 10,
-        2 * flops,
-        room,
-        mib=60,
-    )(ids, *near, *far, wq, wg)
-    q = lax.all_to_all(qx, "x", 0, 0, tiled=True).reshape(SLAB, 128)
+    same, other = project(query_kernel, (shape(BLOCK, 128),) * 2, (wq,))
+
+    def swap(values):
+        out = [values[0]]
+        for s in range(1, NX):
+            out.append(lax.ppermute(values[s], "x", ring(NX, s)))
+        return out
+
+    qs = swap((same, other, same, other))
+    gate = project(gate_kernel, shape(2, BLOCK, 128, dtype=F32), (wg,))
 
     def hop(value, direction):
         return lax.ppermute(value, "z", ring(NZ, direction))
@@ -421,14 +450,7 @@
     far0 = hop(kf[3][:2], 1)
     far1 = hop(kb[3][2:], -1)
 
-    ids = pl.pallas_call(
-        arrived_kernel,
-        out_shape=shape(4, dtype=jnp.int32),
-        in_specs=[sspec(), hbm, hbm],
-        out_specs=sspec(),
-        name="arrived",
-    )(ids, kf[1], kb[1])
-    qa, *front = attention(diag_kernel, (shape(SLAB, 256), *STATE), 3)(ids, q, kv)
+    qa, *front = attention(diag_kernel, (shape(SLAB, 256), *STATE), 6)(ids, *qs, kv)
     back = []
     for s in range(1, 4):
         back = attention(
@@ -439,10 +461,12 @@
             functools.partial(front_kernel, s), STATE, 6, {3: 0, 4: 1, 5: 2}
         )(ids, qa, kf[s], *front)
     outs = attention(
-        last_kernel, shape(NX, BLOCK + META, 128), 10, None, [VMEM(s.shape, F32) for s in STATE]
+        last_kernel, (shape(BLOCK + META, 128),) * NX, 10, None, [VMEM(s.shape, F32) for s in STATE]
     )(ids, qa, far0, far1, *front, *back)
-    parts = lax.all_to_all(outs, "x", 0, 0, tiled=True)
-    att = call(join_kernel, shape(NY * NC, PIECE, COLS), [vspec()] * 2, 1 << 20)(parts, gate)
+    parts = swap(outs)
+    att = call(
+        join_kernel, shape(NY * NC, PIECE, COLS), [sspec()] + [vspec()] * 5, 1 << 20
+    )(ids, *parts, gate)
     rows = lax.all_to_all(att, ("y", "c"), 0, 0, tiled=True)
     return call(
         out_kernel, shape(PIECE, WIDTH), [vspec()] * 2, 2 * PIECE * WIDTH * WIDTH,

time: 133 us -> 148 us (1.11)
  waiting for transfers between devices: 26.4 us -> 38.5 us
  blocking collectives: 35.7 us -> 25 us
  starting transfers between devices: 18.9 us -> 26.2 us
  local copies, waits for them, and re-layouts: 1.41 us -> 6.07 us
  Pallas kernels: 49.3 us -> 50.9 us
    all_to_all x1 -> x0, blocking collectives: 10.7 us -> none  [body(): parts = lax.all_to_all(outs, 'x', 0, 0, tiled=True)]
    ppermute x8, waiting for transfers between devices: 12.9 us -> 21.5 us  [hop(): return lax.ppermute(value, 'z', ring(NZ, direction))]
    ppermute x4 -> x10, starting transfers between devices: 0.51 us -> 8.47 us  [the longest x6 7.96 us: swap(): out.append(lax.ppermute(values[s], 'x', ring(NX, s)))]
    ppermute x4 -> x10, waiting for transfers between devices: 0.78 us -> 6.54 us  [the longest x6 5.76 us: swap(): out.append(lax.ppermute(values[s], 'x', ring(NX, s)))]
    unnamed x30 -> x24, local copies, waits for them, and re-layouts: 1.37 us -> 6.03 us
    all_to_all x1 -> x0, starting transfers between devices: 3.48 us -> none  [body(): q = lax.all_to_all(qx, 'x', 0, 0, tiled=True).reshape(SLAB, 128)]
    ppermute x8, starting transfers between devices: 9.08 us -> 11.9 us  [hop(): return lax.ppermute(value, 'z', ring(NZ, direction))]
    all_to_all x1 -> x0, waiting for transfers between devices: 2.25 us -> none  [body(): q = lax.all_to_all(qx, 'x', 0, 0, tiled=True).reshape(SLAB, 128)]
  transfers between devices with their start and end apart: 16 -> 21, of which waited for: 7 -> 10; matrix products, arithmetic and copies ran while one was open for 0% -> 0% of each run, Pallas kernels for 27% -> 25%
where the time goes in v1:
time: 148 us; the launch traced here: 147 us
  Pallas kernels  50.9 us (34%)
  waiting for transfers between devices  38.5 us (26%)
  starting transfers between devices  26.2 us (18%)
  blocking collectives  25 us (17%)
  local copies, waits for them, and re-layouts  6.07 us (4%)
    ppermute x8, waiting for transfers between devices, hop(): return lax.ppermute(value, 'z', ring(NZ, direction))  21.5 us
    all_to_all x1, blocking collectives, body(): kv = lax.all_to_all(kvx, 'x', 0, 0, tiled=True)  14.3 us
    pallas_call x3, Pallas kernels, project(): call(kernel, outs, [sspec()] + [hbm] * (8 + len(weights)) + list(specs),...  13.9 us
    pallas_call x3, Pallas kernels, body(): attention(functools.partial(front_kernel, s), STATE, 6, {3: 0, 4: 1, 5: 2})  13.2 us
    pallas_call x3, Pallas kernels, body(): attention(functools.partial(back_kernel, s), STATE, 3 + len(back), {3: 0,...  12.9 us
    ppermute x8, starting transfers between devices, hop(): return lax.ppermute(value, 'z', ring(NZ, direction))  11.9 us
    all_to_all x1, blocking collectives, body(): rows = lax.all_to_all(att, ('y', 'c'), 0, 0, tiled=True)  10.8 us
    ppermute x3, waiting for transfers between devices, body(): lax.ppermute(tokens, 'y', ring(NY, s))  10.5 us
  transfers between devices with their start and end apart: 21, of which 10 were waited for; matrix products, arithmetic and copies ran while one was open for 0% of the time, Pallas kernels for 25%

profile of v1, /device:TPU:224, one launch (start us, length us, event | category | flops | bytes accessed | tf_op | source)
XLA Modules:
  0.0 147.4 jit_solution(16739830488506645350)
XLA Ops:
  0.0 1.6 %collective-permute-start = (bf16[64,2048]{1,0:T(8,128)(2,1)}, bf16[64,2048]{1,0:T(8,128)(2,1)S(1)}, u32[]{:S(2)}, u32[]{:S(2)}) collective-permute-start(bf16[64,2048]{1,0:T(8,128)(2,1)} %refs_0_.5), channel_id=1, source_target_pairs={{0,2},{2,4},{4,6},{6,0},{1,3},{3,5},{5,7},{7,1},{8,10},{10,12},{12... | collective-permute-start | bytes 786440 | tf_op jit(solution)/shard_map/ppermute | solution.py:411
  1.6 2.9 %collective-permute-start.1 = (bf16[64,2048]{1,0:T(8,128)(2,1)}, bf16[64,2048]{1,0:T(8,128)(2,1)S(1)}, u32[]{:S(2)}, u32[]{:S(2)}) collective-permute-start(bf16[64,2048]{1,0:T(8,128)(2,1)} %refs_0_.5), channel_id=1, source_target_pairs={{0,4},{2,6},{4,0},{6,2},{1,5},{3,7},{5,1},{7,3},{8,12},{10,14},{12... | collective-permute-start | bytes 786440 | tf_op jit(solution)/shard_map/ppermute | solution.py:411
  4.5 1.3 collective-permute-start.2
  5.8 3.7 %collective-permute-done.refs_1_ = bf16[64,2048]{1,0:T(8,128)(2,1)S(1)} collective-permute-done((bf16[64,2048]{1,0:T(8,128)(2,1)}, bf16[64,2048]{1,0:T(8,128)(2,1)S(1)}, u32[]{:S(2)}, u32[]{:S(2)}) %collective-permute-start) | collective-permute-done | bytes 262176 | tf_op jit(solution)/shard_map/ppermute | solution.py:411
  9.5 6.8 %collective-permute-done.1.refs_2_ = bf16[64,2048]{1,0:T(8,128)(2,1)S(1)} collective-permute-done((bf16[64,2048]{1,0:T(8,128)(2,1)}, bf16[64,2048]{1,0:T(8,128)(2,1)S(1)}, u32[]{:S(2)}, u32[]{:S(2)}) %collective-permute-start.1) | collective-permute-done | bytes 262176 | tf_op jit(solution)/shard_map/ppermute | solution.py:411
  18.9 5.7 %shard_map.83 = bf16[4,528,128]{2,1,0:T(8,128)(2,1)} custom-call(s32[4]{0:T(128)} %pad_add_fusion.ids_ref, bf16[64,2048]{1,0:T(8,128)(2,1)} %refs_0_.5, bf16[64,2048]{1,0:T(8,128)(2,1)} %copy-done.5, bf16[64,2048]{1,0:T(8,128)(2,1)} %copy-done.6, bf16[64,2048]{1,0:T(8,128)(2,1)} %copy-done.7, bf16[64,2048]{1,0:T(8,128)(2,1)} %copy-done.8, ...), custom_call_target="tpu_custom_call" | custom-call | flops 1073741824 | bytes 2097152 | tf_op jit(solution)/shard_map/pallas_call | solution.py:419
  24.6 14.3 %all_to_all.10.kv_ref = bf16[4,528,128]{2,1,0:T(8,128)(2,1)S(1)} all-to-all(bf16[4,528,128]{2,1,0:T(8,128)(2,1)} %shard_map.83), channel_id=1, replica_groups=mesh['z'=8,'x'=4,'y'=4,'c'=2] {'x'}, dimensions={0} | all-to-all | bytes 1081344 | tf_op jit(solution)/shard_map/all_to_all | solution.py:431
  38.9 1.0 collective-permute-start.14
  39.9 2.2 %collective-permute-start.10 = (bf16[4,528,128]{2,1,0:T(8,128)(2,1)S(1)}, bf16[4,528,128]{2,1,0:T(8,128)(2,1)S(1)}, u32[]{:S(2)}, u32[]{:S(2)}) collective-permute-start(bf16[4,528,128]{2,1,0:T(8,128)(2,1)S(1)} %all_to_all.10.kv_ref), channel_id=1, source_target_pairs={{0,32},{32,64},{64,96},{96,128},{128,160},{160,192},{192,224},{224... | collective-permute-start | bytes 1622024 | tf_op jit(solution)/shard_map/ppermute | solution.py:444
  42.1 11.2 %collective-permute-done.14.kv_ref = bf16[4,528,128]{2,1,0:T(8,128)(2,1)S(1)} collective-permute-done((bf16[4,528,128]{2,1,0:T(8,128)(2,1)S(1)}, bf16[4,528,128]{2,1,0:T(8,128)(2,1)S(1)}, u32[]{:S(2)}, u32[]{:S(2)}) %collective-permute-start.14) | collective-permute-done | bytes 540704 | tf_op jit(solution)/shard_map/ppermute | solution.py:444
  53.3 3.2 %collective-permute-start.11 = (bf16[4,528,128]{2,1,0:T(8,128)(2,1)S(1)}, bf16[4,528,128]{2,1,0:T(8,128)(2,1)S(1)}, u32[]{:S(2)}, u32[]{:S(2)}) collective-permute-start(bf16[4,528,128]{2,1,0:T(8,128)(2,1)S(1)} %collective-permute-done.10.kv_ref), channel_id=1, source_target_pairs={{0,32},{32,64},{64,96},{96,128},{128,160},{160,192},{192,224},{224... | collective-permute-start | bytes 1622024 | tf_op jit(solution)/shard_map/ppermute | solution.py:444
  56.5 10.3 %collective-permute-done.15.kv_ref = bf16[4,528,128]{2,1,0:T(8,128)(2,1)S(1)} collective-permute-done((bf16[4,528,128]{2,1,0:T(8,128)(2,1)S(1)}, bf16[4,528,128]{2,1,0:T(8,128)(2,1)S(1)}, u32[]{:S(2)}, u32[]{:S(2)}) %collective-permute-start.15) | collective-permute-done | bytes 540704 | tf_op jit(solution)/shard_map/ppermute | solution.py:444
  66.8 3.2 %collective-permute-start.12 = (bf16[4,528,128]{2,1,0:T(8,128)(2,1)S(1)}, bf16[4,528,128]{2,1,0:T(8,128)(2,1)S(1)}, u32[]{:S(2)}, u32[]{:S(2)}) collective-permute-start(bf16[4,528,128]{2,1,0:T(8,128)(2,1)S(1)} %collective-permute-done.11.kv_ref), channel_id=1, source_target_pairs={{0,32},{32,64},{64,96},{96,128},{128,160},{160,192},{192,224},{224... | collective-permute-start | bytes 1622024 | tf_op jit(solution)/shard_map/ppermute | solution.py:444
  70.1 4.1 %shard_map.82 = (bf16[512,128]{1,0:T(8,128)(2,1)}, bf16[512,128]{1,0:T(8,128)(2,1)}) custom-call(s32[4]{0:T(128)} %pad_add_fusion.ids_ref, bf16[64,2048]{1,0:T(8,128)(2,1)} %refs_0_.5, bf16[64,2048]{1,0:T(8,128)(2,1)} %copy-done.5, bf16[64,2048]{1,0:T(8,128)(2,1)} %copy-done.6, bf16[64,2048]{1,0:T(8,128)(2,1)} %copy-done.7, bf16[64,2048]{1,0:T(8,128)(2,1)} %copy-done.8, ...), custom_call_target="tpu_custom_call" | custom-call | flops 536870912 | bytes 2097152 | tf_op jit(solution)/shard_map/pallas_call | solution.py:419
  74.8 2.1 %collective-permute-start.8 = (bf16[512,128]{1,0:T(8,128)(2,1)}, bf16[512,128]{1,0:T(8,128)(2,1)S(1)}, u32[]{:S(2)}, u32[]{:S(2)}) collective-permute-start(bf16[512,128]{1,0:T(8,128)(2,1)} %get-tuple-element.33.q0), channel_id=1, source_target_pairs={{0,16},{8,24},{16,0},{24,8},{1,17},{9,25},{17,1},{25,9},{2,18},{10... | collective-permute-start | bytes 393224 | tf_op jit(solution)/shard_map/ppermute | solution.py:437
  76.8 1.0 collective-permute-start.9
  77.9 4.1 %collective-permute-done.7.q1 = bf16[512,128]{1,0:T(8,128)(2,1)S(1)} collective-permute-done((bf16[512,128]{1,0:T(8,128)(2,1)}, bf16[512,128]{1,0:T(8,128)(2,1)S(1)}, u32[]{:S(2)}, u32[]{:S(2)}) %collective-permute-start.7) | collective-permute-done | bytes 131104 | tf_op jit(solution)/shard_map/ppermute | solution.py:437
  83.8 3.2 %shard_map.84 = (bf16[2048,256]{1,0:T(8,128)(2,1)S(1)}, f32[8,128]{1,0:T(8,128)S(1)}, f32[8,8,256]{2,1,0:T(8,128)S(1)}, f32[8,144,256]{2,1,0:T(8,128)S(1)}) custom-call(s32[4]{0:T(128)S(1)} %copy-done.2, bf16[512,128]{1,0:T(8,128)(2,1)S(1)} %copy-done.4, bf16[512,128]{1,0:T(8,128)(2,1)S(1)} %collective-permute-done.7.q1, ...), custom_call_target="tpu_custom_call" | custom-call | flops 1073741824 | bytes 2097152 | tf_op jit(solution)/shard_map/pallas_call | solution.py:453
  86.9 4.2 %shard_map.88 = (f32[8,128]{1,0:T(8,128)S(1)}, f32[8,8,256]{2,1,0:T(8,128)S(1)}, f32[8,144,256]{2,1,0:T(8,128)S(1)}) custom-call(s32[4]{0:T(128)S(1)} %copy-done.2, bf16[2048,256]{1,0:T(8,128)(2,1)S(1)} %get-tuple-element.35.qa_ref, bf16[4,528,128]{2,1,0:T(8,128)(2,1)S(1)} %collective-permute-done.14.kv_ref), custom_call_target="tpu_custom_call" | custom-call | flops 1073741824 | bytes 2097152 | tf_op jit(solution)/shard_map/pallas_call | solution.py:456
  91.2 4.3 %shard_map.85 = (f32[8,128]{1,0:T(8,128)S(1)}, f32[8,8,256]{2,1,0:T(8,128)S(1)}, f32[8,144,256]{2,1,0:T(8,128)S(1)}) custom-call(s32[4]{0:T(128)S(1)} %copy-done.2, bf16[2048,256]{1,0:T(8,128)(2,1)S(1)} %get-tuple-element.35.qa_ref, ...), custom_call_target="tpu_custom_call", output_to_operand_aliasing={{0}: (3, {}), {1}: (4, {}), {2}: (5, {})} | custom-call | flops 1073741824 | bytes 2097152 | tf_op jit(solution)/shard_map/pallas_call | solution.py:460
  95.5 4.3 %shard_map.89 = (f32[8,128]{1,0:T(8,128)S(1)}, f32[8,8,256]{2,1,0:T(8,128)S(1)}, f32[8,144,256]{2,1,0:T(8,128)S(1)}) custom-call(s32[4]{0:T(128)S(1)} %copy-done.2, bf16[2048,256]{1,0:T(8,128)(2,1)S(1)} %get-tuple-element.35.qa_ref, ...), custom_call_target="tpu_custom_call", output_to_operand_aliasing={{0}: (3, {}), {1}: (4, {}), {2}: (5, {})} | custom-call | flops 1073741824 | bytes 2097152 | tf_op jit(solution)/shard_map/pallas_call | solution.py:456
  100.0 2.1 %collective-permute-start.17 = (bf16[2,528,128]{2,1,0:T(8,128)(2,1)S(1)}, bf16[2,528,128]{2,1,0:T(8,128)(2,1)S(1)}, u32[]{:S(2)}, u32[]{:S(2)}) collective-permute-start(bf16[2,528,128]{2,1,0:T(8,128)(2,1)S(1)} %slice.9), channel_id=1, source_target_pairs={{0,224},{32,0},{64,32},{96,64},{128,96},{160,128},{192,160},{224,1... | collective-permute-start | bytes 811016 | tf_op jit(solution)/shard_map/ppermute | solution.py:444
  102.1 4.5 %shard_map.86 = (f32[8,128]{1,0:T(8,128)S(1)}, f32[8,8,256]{2,1,0:T(8,128)S(1)}, f32[8,144,256]{2,1,0:T(8,128)S(1)}) custom-call(s32[4]{0:T(128)S(1)} %copy-done.2, bf16[2048,256]{1,0:T(8,128)(2,1)S(1)} %get-tuple-element.35.qa_ref, ...), custom_call_target="tpu_custom_call", output_to_operand_aliasing={{0}: (3, {}), {1}: (4, {}), {2}: (5, {})} | custom-call | flops 1073741824 | bytes 2097152 | tf_op jit(solution)/shard_map/pallas_call | solution.py:460
  106.6 4.3 %shard_map.90 = (f32[8,128]{1,0:T(8,128)S(1)}, f32[8,8,256]{2,1,0:T(8,128)S(1)}, f32[8,144,256]{2,1,0:T(8,128)S(1)}) custom-call(s32[4]{0:T(128)S(1)} %copy-done.2, bf16[2048,256]{1,0:T(8,128)(2,1)S(1)} %get-tuple-element.35.qa_ref, ...), custom_call_target="tpu_custom_call", output_to_operand_aliasing={{0}: (3, {}), {1}: (4, {}), {2}: (5, {})} | custom-call | flops 1073741824 | bytes 2097152 | tf_op jit(solution)/shard_map/pallas_call | solution.py:456
  111.0 4.3 %shard_map.87 = (f32[8,128]{1,0:T(8,128)S(1)}, f32[8,8,256]{2,1,0:T(8,128)S(1)}, f32[8,144,256]{2,1,0:T(8,128)S(1)}) custom-call(s32[4]{0:T(128)S(1)} %copy-done.2, bf16[2048,256]{1,0:T(8,128)(2,1)S(1)} %get-tuple-element.35.qa_ref, ...), custom_call_target="tpu_custom_call", output_to_operand_aliasing={{0}: (3, {}), {1}: (4, {}), {2}: (5, {})} | custom-call | flops 1073741824 | bytes 2097152 | tf_op jit(solution)/shard_map/pallas_call | solution.py:460
  115.3 4.6 %shard_map.91 = (bf16[528,128]{1,0:T(8,128)(2,1)S(1)}, bf16[528,128]{1,0:T(8,128)(2,1)S(1)}, bf16[528,128]{1,0:T(8,128)(2,1)S(1)}, bf16[528,128]{1,0:T(8,128)(2,1)S(1)}) custom-call(s32[4]{0:T(128)S(1)} %copy-done.2, bf16[2048,256]{1,0:T(8,128)(2,1)S(1)} %get-tuple-element.35.qa_ref, bf16[2,528,128]{2,1,0:T(8,128)(2,1)S(1)} %collective-permute-done.13.kv0_ref, ...), custom_call_target="tpu_custom_call" | custom-call | flops 1073741824 | bytes 2097152 | tf_op jit(solution)/shard_map/pallas_call | solution.py:463
  120.6 3.5 %collective-permute-start.19 = (bf16[528,128]{1,0:T(8,128)(2,1)S(1)}, bf16[528,128]{1,0:T(8,128)(2,1)S(1)}, u32[]{:S(2)}, u32[]{:S(2)}) collective-permute-start(bf16[528,128]{1,0:T(8,128)(2,1)S(1)} %get-tuple-element.59), channel_id=1, source_target_pairs={{0,16},{8,24},{16,0},{24,8},{1,17},{9,25},{17,1},{25,9},{2,18},{10... | collective-permute-start | bytes 405512 | tf_op jit(solution)/shard_map/ppermute | solution.py:437
  124.2 4.2 %shard_map.92.gate_ref = f32[2,512,128]{2,1,0:T(8,128)} custom-call(s32[4]{0:T(128)} %pad_add_fusion.ids_ref, bf16[64,2048]{1,0:T(8,128)(2,1)} %refs_0_.5, bf16[64,2048]{1,0:T(8,128)(2,1)} %copy-done.5, bf16[64,2048]{1,0:T(8,128)(2,1)} %copy-done.6, bf16[64,2048]{1,0:T(8,128)(2,1)} %copy-done.7, bf16[64,2048]{1,0:T(8,128)(2,1)} %copy-done.8, ...), custom_call_target="tpu_custom_call" | custom-call | flops 536870912 | bytes 2097152 | tf_op jit(solution)/shard_map/pallas_call | solution.py:419
  129.2 1.0 copy-done.1
  131.0 10.8 %all_to_all.11.rows_ref = bf16[8,64,256]{2,1,0:T(8,128)(2,1)S(1)} all-to-all(bf16[8,64,256]{2,1,0:T(8,128)(2,1)S(1)} %shard_map.93), channel_id=1, replica_groups=mesh['z'=8,'x'=4,'y'=4,'c'=2] {'y','c'}, dimensions={0} | all-to-all | bytes 524288 | tf_op jit(solution)/shard_map/all_to_all | solution.py:470
  141.8 3.4 %copy-done = bf16[2048,2048]{1,0:T(8,128)(2,1)S(1)} copy-done((bf16[2048,2048]{1,0:T(8,128)(2,1)S(1)}, bf16[2048,2048]{1,0:T(8,128)(2,1)}, u32[]{:S(2)}) %copy-start) | copy-done | bytes 8388632
  145.2 2.3 %shard_map.94 = bf16[64,2048]{1,0:T(8,128)(2,1)} custom-call(bf16[8,64,256]{2,1,0:T(8,128)(2,1)S(1)} %all_to_all.11.rows_ref, bf16[2048,2048]{1,0:T(8,128)(2,1)S(1)} %copy-done), custom_call_target="tpu_custom_call" | custom-call | flops 536870912 | bytes 2097152 | tf_op jit(solution)/shard_map/pallas_call | solution.py:471
  (52 shorter events, 7.4 us)
Async XLA Ops:
  0.0 9.5 %collective-permute-start = (bf16[64,2048]{1,0:T(8,128)(2,1)}, bf16[64,2048]{1,0:T(8,128)(2,1)S(1)}, u32[]{:S(2)}, u32[]{:S(2)}) collective-permute-start(bf16[64,2048]{1,0:T(8,128)(2,1)} %refs_0_.5), channel_id=1, source_target_pairs={{0,2},{2,4},{4,6},{6,0},{1,3},{3,5},{5,7},{7,1},{8,10},{10,12},{12... | collective-permute-start | bytes 786440 | tf_op jit(solution)/shard_map/ppermute | solution.py:411
  1.6 14.7 %collective-permute-start.1 = (bf16[64,2048]{1,0:T(8,128)(2,1)}, bf16[64,2048]{1,0:T(8,128)(2,1)S(1)}, u32[]{:S(2)}, u32[]{:S(2)}) collective-permute-start(bf16[64,2048]{1,0:T(8,128)(2,1)} %refs_0_.5), channel_id=1, source_target_pairs={{0,4},{2,6},{4,0},{6,2},{1,5},{3,7},{5,1},{7,3},{8,12},{10,14},{12... | collective-permute-start | bytes 786440 | tf_op jit(solution)/shard_map/ppermute | solution.py:411
  4.5 11.9 %collective-permute-start.2 = (bf16[64,2048]{1,0:T(8,128)(2,1)}, bf16[64,2048]{1,0:T(8,128)(2,1)S(1)}, u32[]{:S(2)}, u32[]{:S(2)}) collective-permute-start(bf16[64,2048]{1,0:T(8,128)(2,1)} %refs_0_.5), channel_id=1, source_target_pairs={{0,6},{2,0},{4,2},{6,4},{1,7},{3,1},{5,3},{7,5},{8,14},{10,8},{12,... | collective-permute-start | bytes 786440 | tf_op jit(solution)/shard_map/ppermute | solution.py:411
  5.8 11.6 %collective-permute-start.3 = (bf16[64,2048]{1,0:T(8,128)(2,1)}, bf16[64,2048]{1,0:T(8,128)(2,1)S(1)}, u32[]{:S(2)}, u32[]{:S(2)}) collective-permute-start(bf16[64,2048]{1,0:T(8,128)(2,1)} %refs_0_.5), channel_id=1, source_target_pairs={{0,1},{1,0},{2,3},{3,2},{4,5},{5,4},{6,7},{7,6},{8,9},{9,8},{10,11... | collective-permute-start | bytes 786440 | tf_op jit(solution)/shard_map/ppermute | solution.py:412
  9.5 8.7 %copy-start.5 = (bf16[64,2048]{1,0:T(8,128)(2,1)}, bf16[64,2048]{1,0:T(8,128)(2,1)S(1)}, u32[]{:S(2)}) copy-start(bf16[64,2048]{1,0:T(8,128)(2,1)S(1)} %collective-permute-done.refs_1_) | copy-start | bytes 786436
  9.5 7.9 %collective-permute-start.4 = (bf16[64,2048]{1,0:T(8,128)(2,1)S(1)}, bf16[64,2048]{1,0:T(8,128)(2,1)S(1)}, u32[]{:S(2)}, u32[]{:S(2)}) collective-permute-start(bf16[64,2048]{1,0:T(8,128)(2,1)S(1)} %collective-permute-done.refs_1_), channel_id=1, source_target_pairs={{0,1},{1,0},{2,3},{3,2},{4,5},{5,4},{6,7},{7,6},{8,9},{9,8},{10,11... | collective-permute-start | bytes 786440 | tf_op jit(solution)/shard_map/ppermute | solution.py:413
  16.3 1.9 %copy-start.6 = (bf16[64,2048]{1,0:T(8,128)(2,1)}, bf16[64,2048]{1,0:T(8,128)(2,1)S(1)}, u32[]{:S(2)}) copy-start(bf16[64,2048]{1,0:T(8,128)(2,1)S(1)} %collective-permute-done.1.refs_2_) | copy-start | bytes 786436
  16.3 1.5 %collective-permute-start.5 = (bf16[64,2048]{1,0:T(8,128)(2,1)S(1)}, bf16[64,2048]{1,0:T(8,128)(2,1)S(1)}, u32[]{:S(2)}, u32[]{:S(2)}) collective-permute-start(bf16[64,2048]{1,0:T(8,128)(2,1)S(1)} %collective-permute-done.1.refs_2_), channel_id=1, source_target_pairs={{0,1},{1,0},{2,3},{3,2},{4,5},{5,4},{6,7},{7,6},{8,9},{9,8},{10,11... | collective-permute-start | bytes 786440 | tf_op jit(solution)/shard_map/ppermute | solution.py:413
  16.3 1.9 %copy-start.7 = (bf16[64,2048]{1,0:T(8,128)(2,1)}, bf16[64,2048]{1,0:T(8,128)(2,1)S(1)}, u32[]{:S(2)}) copy-start(bf16[64,2048]{1,0:T(8,128)(2,1)S(1)} %collective-permute-done.2.refs_3_) | copy-start | bytes 786436
  16.3 1.9 %collective-permute-start.6 = (bf16[64,2048]{1,0:T(8,128)(2,1)S(1)}, bf16[64,2048]{1,0:T(8,128)(2,1)S(1)}, u32[]{:S(2)}, u32[]{:S(2)}) collective-permute-start(bf16[64,2048]{1,0:T(8,128)(2,1)S(1)} %collective-permute-done.2.refs_3_), channel_id=1, source_target_pairs={{0,1},{1,0},{2,3},{3,2},{4,5},{5,4},{6,7},{7,6},{8,9},{9,8},{10,11... | collective-permute-start | bytes 786440 | tf_op jit(solution)/shard_map/ppermute | solution.py:413
  17.4 0.8 copy-start.8
  17.4 0.8 copy-start.9
  18.2 0.7 copy-start.11
  38.9 44.0 %copy-start.2 = (s32[4]{0:T(128)S(1)}, s32[4]{0:T(128)}, u32[]{:S(2)}) copy-start(s32[4]{0:T(128)} %pad_add_fusion.ids_ref) | copy-start | bytes 52
  38.9 14.4 %collective-permute-start.14 = (bf16[4,528,128]{2,1,0:T(8,128)(2,1)S(1)}, bf16[4,528,128]{2,1,0:T(8,128)(2,1)S(1)}, u32[]{:S(2)}, u32[]{:S(2)}) collective-permute-start(bf16[4,528,128]{2,1,0:T(8,128)(2,1)S(1)} %all_to_all.10.kv_ref), channel_id=1, source_target_pairs={{0,224},{32,0},{64,32},{96,64},{128,96},{160,128},{192,160},{224,1... | collective-permute-start | bytes 1622024 | tf_op jit(solution)/shard_map/ppermute | solution.py:444
  39.9 13.4 %collective-permute-start.10 = (bf16[4,528,128]{2,1,0:T(8,128)(2,1)S(1)}, bf16[4,528,128]{2,1,0:T(8,128)(2,1)S(1)}, u32[]{:S(2)}, u32[]{:S(2)}) collective-permute-start(bf16[4,528,128]{2,1,0:T(8,128)(2,1)S(1)} %all_to_all.10.kv_ref), channel_id=1, source_target_pairs={{0,32},{32,64},{64,96},{96,128},{128,160},{160,192},{192,224},{224... | collective-permute-start | bytes 1622024 | tf_op jit(solution)/shard_map/ppermute | solution.py:444
  53.3 13.5 %collective-permute-start.15 = (bf16[4,528,128]{2,1,0:T(8,128)(2,1)S(1)}, bf16[4,528,128]{2,1,0:T(8,128)(2,1)S(1)}, u32[]{:S(2)}, u32[]{:S(2)}) collective-permute-start(bf16[4,528,128]{2,1,0:T(8,128)(2,1)S(1)} %collective-permute-done.14.kv_ref), channel_id=1, source_target_pairs={{0,224},{32,0},{64,32},{96,64},{128,96},{160,128},{192,160},{224,1... | collective-permute-start | bytes 1622024 | tf_op jit(solution)/shard_map/ppermute | solution.py:444
  53.3 13.5 %collective-permute-start.11 = (bf16[4,528,128]{2,1,0:T(8,128)(2,1)S(1)}, bf16[4,528,128]{2,1,0:T(8,128)(2,1)S(1)}, u32[]{:S(2)}, u32[]{:S(2)}) collective-permute-start(bf16[4,528,128]{2,1,0:T(8,128)(2,1)S(1)} %collective-permute-done.10.kv_ref), channel_id=1, source_target_pairs={{0,32},{32,64},{64,96},{96,128},{128,160},{160,192},{192,224},{224... | collective-permute-start | bytes 1622024 | tf_op jit(solution)/shard_map/ppermute | solution.py:444
  66.8 33.1 %collective-permute-start.16 = (bf16[4,528,128]{2,1,0:T(8,128)(2,1)S(1)}, bf16[4,528,128]{2,1,0:T(8,128)(2,1)S(1)}, u32[]{:S(2)}, u32[]{:S(2)}) collective-permute-start(bf16[4,528,128]{2,1,0:T(8,128)(2,1)S(1)} %collective-permute-done.15.kv_ref), channel_id=1, source_target_pairs={{0,224},{32,0},{64,32},{96,64},{128,96},{160,128},{192,160},{224,1... | collective-permute-start | bytes 1622024 | tf_op jit(solution)/shard_map/ppermute | solution.py:444
  66.8 33.0 %collective-permute-start.12 = (bf16[4,528,128]{2,1,0:T(8,128)(2,1)S(1)}, bf16[4,528,128]{2,1,0:T(8,128)(2,1)S(1)}, u32[]{:S(2)}, u32[]{:S(2)}) collective-permute-start(bf16[4,528,128]{2,1,0:T(8,128)(2,1)S(1)} %collective-permute-done.11.kv_ref), channel_id=1, source_target_pairs={{0,32},{32,64},{64,96},{96,128},{128,160},{160,192},{192,224},{224... | collective-permute-start | bytes 1622024 | tf_op jit(solution)/shard_map/ppermute | solution.py:444
  74.1 7.9 %collective-permute-start.7 = (bf16[512,128]{1,0:T(8,128)(2,1)}, bf16[512,128]{1,0:T(8,128)(2,1)S(1)}, u32[]{:S(2)}, u32[]{:S(2)}) collective-permute-start(bf16[512,128]{1,0:T(8,128)(2,1)} %get-tuple-element.34), channel_id=1, source_target_pairs={{0,8},{8,16},{16,24},{24,0},{1,9},{9,17},{17,25},{25,1},{2,10},{10... | collective-permute-start | bytes 393224 | tf_op jit(solution)/shard_map/ppermute | solution.py:437
  74.8 7.2 %collective-permute-start.8 = (bf16[512,128]{1,0:T(8,128)(2,1)}, bf16[512,128]{1,0:T(8,128)(2,1)S(1)}, u32[]{:S(2)}, u32[]{:S(2)}) collective-permute-start(bf16[512,128]{1,0:T(8,128)(2,1)} %get-tuple-element.33.q0), channel_id=1, source_target_pairs={{0,16},{8,24},{16,0},{24,8},{1,17},{9,25},{17,1},{25,9},{2,18},{10... | collective-permute-start | bytes 393224 | tf_op jit(solution)/shard_map/ppermute | solution.py:437
  76.8 6.0 %collective-permute-start.9 = (bf16[512,128]{1,0:T(8,128)(2,1)}, bf16[512,128]{1,0:T(8,128)(2,1)S(1)}, u32[]{:S(2)}, u32[]{:S(2)}) collective-permute-start(bf16[512,128]{1,0:T(8,128)(2,1)} %get-tuple-element.34), channel_id=1, source_target_pairs={{0,24},{8,0},{16,8},{24,16},{1,25},{9,1},{17,9},{25,17},{2,26},{10... | collective-permute-start | bytes 393224 | tf_op jit(solution)/shard_map/ppermute | solution.py:437
  82.9 0.9 copy-start.4
  99.9 15.4 %collective-permute-start.13 = (bf16[2,528,128]{2,1,0:T(8,128)(2,1)S(1)}, bf16[2,528,128]{2,1,0:T(8,128)(2,1)S(1)}, u32[]{:S(2)}, u32[]{:S(2)}) collective-permute-start(bf16[2,528,128]{2,1,0:T(8,128)(2,1)S(1)} %slice.8), channel_id=1, source_target_pairs={{0,32},{32,64},{64,96},{96,128},{128,160},{160,192},{192,224},{224... | collective-permute-start | bytes 811016 | tf_op jit(solution)/shard_map/ppermute | solution.py:444
  100.0 15.3 %collective-permute-start.17 = (bf16[2,528,128]{2,1,0:T(8,128)(2,1)S(1)}, bf16[2,528,128]{2,1,0:T(8,128)(2,1)S(1)}, u32[]{:S(2)}, u32[]{:S(2)}) collective-permute-start(bf16[2,528,128]{2,1,0:T(8,128)(2,1)S(1)} %slice.9), channel_id=1, source_target_pairs={{0,224},{32,0},{64,32},{96,64},{128,96},{160,128},{192,160},{224,1... | collective-permute-start | bytes 811016 | tf_op jit(solution)/shard_map/ppermute | solution.py:444
  119.9 8.4 %collective-permute-start.18 = (bf16[528,128]{1,0:T(8,128)(2,1)S(1)}, bf16[528,128]{1,0:T(8,128)(2,1)S(1)}, u32[]{:S(2)}, u32[]{:S(2)}) collective-permute-start(bf16[528,128]{1,0:T(8,128)(2,1)S(1)} %get-tuple-element.58), channel_id=1, source_target_pairs={{0,8},{8,16},{16,24},{24,0},{1,9},{9,17},{17,25},{25,1},{2,10},{10... | collective-permute-start | bytes 405512 | tf_op jit(solution)/shard_map/ppermute | solution.py:437
  120.6 8.0 %collective-permute-start.19 = (bf16[528,128]{1,0:T(8,128)(2,1)S(1)}, bf16[528,128]{1,0:T(8,128)(2,1)S(1)}, u32[]{:S(2)}, u32[]{:S(2)}) collective-permute-start(bf16[528,128]{1,0:T(8,128)(2,1)S(1)} %get-tuple-element.59), channel_id=1, source_target_pairs={{0,16},{8,24},{16,0},{24,8},{1,17},{9,25},{17,1},{25,9},{2,18},{10... | collective-permute-start | bytes 405512 | tf_op jit(solution)/shard_map/ppermute | solution.py:437
  124.2 5.0 %copy-start.3 = (s32[4]{0:T(128)S(1)}, s32[4]{0:T(128)}, u32[]{:S(2)}) copy-start(s32[4]{0:T(128)} %pad_add_fusion.ids_ref) | copy-start | bytes 52
  124.2 5.0 %collective-permute-start.20 = (bf16[528,128]{1,0:T(8,128)(2,1)S(1)}, bf16[528,128]{1,0:T(8,128)(2,1)S(1)}, u32[]{:S(2)}, u32[]{:S(2)}) collective-permute-start(bf16[528,128]{1,0:T(8,128)(2,1)S(1)} %get-tuple-element.60), channel_id=1, source_target_pairs={{0,24},{8,0},{16,8},{24,16},{1,25},{9,1},{17,9},{25,17},{2,26},{10... | collective-permute-start | bytes 405512 | tf_op jit(solution)/shard_map/ppermute | solution.py:437
  129.2 1.0 copy-start.1
  141.8 3.4 %copy-start = (bf16[2048,2048]{1,0:T(8,128)(2,1)S(1)}, bf16[2048,2048]{1,0:T(8,128)(2,1)}, u32[]{:S(2)}) copy-start(bf16[2048,2048]{1,0:T(8,128)(2,1)} %wo_ref.1) | copy-start | bytes 25165828
  (1 other events, 0.7 us)

commit v2 on v1

--- a/solution.py
+++ b/solution.py
@@ -137,7 +137,7 @@
     gate_ref[0], gate_ref[1] = by_parity(ids_ref, 1.0 / (1.0 + jnp.exp(-pre)))
 
 
-QT = 256
+QT = 512
 KEYS = NX * HALF
 TILES = SLAB // QT
 ACC = 144
@@ -169,14 +169,13 @@
     return out, before
 
 
-def attend(qa_ref, ka_ref, vt_ref, half, old, new):
+def attend(qa_ref, ka_ref, vt_ref, half, old, new, d):
     m_out, acc_out = new
 
     def scores(i, keys):
-        start = i * QT if half is not None else pl.multiple_of(i * QT, QT)
         s = lax.dot_general(
             ka_ref[:keys, :],
-            qa_ref[pl.ds(start, QT), :],
+            qa_ref[i * QT : (i + 1) * QT, :],
             (((1,), (1,)), ((), ())),
             preferred_element_type=F32,
         )
@@ -184,39 +183,37 @@
             row = lax.broadcasted_iota(jnp.int32, (keys, QT), 0)
             col = lax.broadcasted_iota(jnp.int32, (keys, QT), 1)
             pos = row + (row // HALF + half) * HALF
-            s = jnp.where(pos <= col + start, s, NEG)
+            s = jnp.where(pos <= col + i * QT, s, NEG)
         return s
 
-    def finish(i, keys, s):
+    def weigh(i, keys, s):
         best = jnp.max(s, axis=0, keepdims=True)
+        factor = None
         if old is not None:
-            before = old[0][i][:1]
+            before = old[0][d, i][:1]
             best = jnp.maximum(best, before)
         safe = jnp.where(best < -1e29, 0.0, best)
-        w = jnp.exp(s - safe).astype(BF)
+        if old is not None:
+            factor = jnp.exp(before - safe)
+        m_out[d, i] = jnp.broadcast_to(best, (8, QT))
+        return i, keys, jnp.exp(s - safe).astype(BF), factor
+
+    def finish(i, keys, w, factor):
         acc = jnp.dot(vt_ref[:, :keys], w, preferred_element_type=F32)
         if old is not None:
-            acc = acc + old[1][i] * jnp.exp(before - safe)
-        m_out[i] = jnp.broadcast_to(best, (8, QT))
-        acc_out[i] = acc
-
-    def run(tiles):
-        s = scores(*tiles[0])
-        for tile, after in zip(tiles, [*tiles[1:], None]):
-            following = scores(*after) if after else None
-            finish(*tile, s)
-            s = following
-
-    if half is not None:
-        run([(i, HALF * (i * QT // BLOCK + 1)) for i in range(TILES)])
-    else:
-        part = TILES // 2
-
-        def some(j, carry):
-            run([(j * part + i, KEYS) for i in range(part)])
-            return carry
-
-        lax.fori_loop(0, 2, some, 0)
+            acc = acc + old[1][d, i] * factor
+        acc_out[d, i] = acc
+
+    tiles = [(i, KEYS if half is None else HALF * (i * QT // BLOCK + 1)) for i in range(TILES)]
+    s = scores(*tiles[0])
+    last = None
+    for tile, after in zip(tiles, [*tiles[1:], None]):
+        following = scores(*after) if after else None
+        if last is not None:
+            finish(*last)
+        last = weigh(*tile, s)
+        s = following
+    finish(*last)
 
 
 def whole(ref):
@@ -231,61 +228,59 @@
         block = (ids_ref[1] + NX - step) % NX
         qa_out[pl.ds(pl.multiple_of(block * BLOCK, BLOCK), BLOCK), :128] = q_ref[...]
     qa_out[:, 128:] = jnp.where(lane < 24, 1.0, 0.0).astype(BF)
-    attend(qa_out, ka_ref, vt_ref, ids_ref[1] // 2, None, (m_out, acc_out))
-    off_out[...] = jnp.zeros((8, 128), F32)
+    attend(qa_out, ka_ref, vt_ref, ids_ref[1] // 2, None, (m_out, acc_out), FRONT)
+    off_out[...] = jnp.zeros(off_out.shape, F32)
+    m_out[BACK] = jnp.full(m_out.shape[1:], NEG, F32)
+    acc_out[BACK] = jnp.zeros(acc_out.shape[1:], F32)
 
 
 def shifted(offsets, base):
     return [(rows, before + base) for rows, before in offsets]
 
 
-def front_kernel(
-    step, ids_ref, qa_ref, kv_ref, off_in, m_in, acc_in, off_out, m_out, acc_out, ka_ref, vt_ref
+BACK, FRONT = 0, 1
+
+
+def step_kernel(
+    step, ids_ref, qa_ref, back_ref, front_ref, off_in, m_in, acc_in, off_out, m_out, acc_out,
+    ka_ref, vt_ref,
 ):
-    valid = ids_ref[0] >= step
-
-    @pl.when(valid)
-    def _():
-        offsets, total = slab_offsets(whole(kv_ref))
-        base = off_in[:1, :] - total
-        fill(whole(kv_ref), shifted(offsets, base), ka_ref, vt_ref)
-        attend(qa_ref, ka_ref, vt_ref, None, (m_in, acc_in), (m_out, acc_out))
-        off_out[...] = jnp.broadcast_to(base, (8, 128))
-
-    @pl.when(jnp.logical_not(valid))
-    def _():
-        off_out[...] = off_in[...]
-        m_out[...] = m_in[...]
-        acc_out[...] = acc_in[...]
-
-
-def back_kernel(step, ids_ref, qa_ref, kv_ref, *refs):
-    ins, (off_out, m_out, acc_out, ka_ref, vt_ref) = refs[:-5], refs[-5:]
-    valid = ids_ref[0] + step >= NZ
-
-    @pl.when(valid)
-    def _():
-        offsets, total = slab_offsets(whole(kv_ref))
-        base = ins[0][:1, :] if ins else jnp.zeros((1, 128), F32)
-        fill(whole(kv_ref), shifted(offsets, base), ka_ref, vt_ref)
-        old = (ins[1], ins[2]) if ins else None
-        attend(qa_ref, ka_ref, vt_ref, None, old, (m_out, acc_out))
-        off_out[...] = jnp.broadcast_to(base + total, (8, 128))
-
-    @pl.when(jnp.logical_not(valid))
-    def _():
-        if ins:
-            off_out[...] = ins[0][...]
-            m_out[...] = ins[1][...]
-            acc_out[...] = ins[2][...]
-        else:
-            off_out[...] = jnp.zeros((8, 128), F32)
-            m_out[...] = jnp.full(m_out.shape, NEG, F32)
-            acc_out[...] = jnp.zeros(acc_out.shape, F32)
+    z = ids_ref[0]
+
+    def one(d, carry):
+        valid = jnp.where(d == BACK, z + step >= NZ, z >= step)
+
+        @pl.when(valid)
+        def _():
+            @pl.when(d == BACK)
+            def _():
+                offsets, total = slab_offsets(whole(back_ref))
+                base = off_in[BACK, :1, :]
+                fill(whole(back_ref), shifted(offsets, base), ka_ref, vt_ref)
+                off_out[BACK] = jnp.broadcast_to(base + total, (8, 128))
+
+            @pl.when(d == FRONT)
+            def _():
+                offsets, total = slab_offsets(whole(front_ref))
+                base = off_in[FRONT, :1, :] - total
+                fill(whole(front_ref), shifted(offsets, base), ka_ref, vt_ref)
+                off_out[FRONT] = jnp.broadcast_to(base, (8, 128))
+
+            attend(qa_ref, ka_ref, vt_ref, None, (m_in, acc_in), (m_out, acc_out), d)
+
+        @pl.when(jnp.logical_not(valid))
+        def _():
+            off_out[d] = off_in[d]
+            m_out[d] = m_in[d]
+            acc_out[d] = acc_in[d]
+
+        return carry
+
+    lax.fori_loop(0, 2, one, 0)
 
 
 def last_kernel(
-    ids_ref, qa_ref, kv0_ref, kv1_ref, foff, fm, facc, boff, bm, bacc, out0, out1, out2, out3,
+    ids_ref, qa_ref, kv0_ref, kv1_ref, off_in, m_in, acc_in, out0, out1, out2, out3,
     off_s, m_s, acc_s, ka_ref, vt_ref,
 ):
     valid = ids_ref[0] >= 4
@@ -294,24 +289,24 @@
     @pl.when(valid)
     def _():
         offsets, total = slab_offsets(blocks)
-        base = foff[:1, :] - total
+        base = off_in[FRONT, :1, :] - total
         fill(blocks, shifted(offsets, base), ka_ref, vt_ref)
-        attend(qa_ref, ka_ref, vt_ref, None, (fm, facc), (m_s, acc_s))
+        attend(qa_ref, ka_ref, vt_ref, None, (m_in, acc_in), (m_s, acc_s), FRONT)
         off_s[...] = jnp.broadcast_to(base, (8, 128))
 
     @pl.when(jnp.logical_not(valid))
     def _():
-        off_s[...] = foff[...]
-        m_s[...] = fm[...]
-        acc_s[...] = facc[...]
-
-    shift = (boff[:1, :] - off_s[:1, :])[:, :1]
+        off_s[...] = off_in[FRONT]
+        m_s[FRONT] = m_in[FRONT]
+        acc_s[FRONT] = acc_in[FRONT]
+
+    shift = (off_in[BACK, :1, :] - off_s[:1, :])[:, :1]
     per = BLOCK // QT
     for step, out_ref in enumerate((out0, out1, out2, out3)):
         block = (ids_ref[1] + step) % NX
         stats = []
         for t in range(per):
-            stats += merge(block * per + t, t, shift, (m_s, acc_s), (bm, bacc), out_ref)
+            stats += merge(block * per + t, t, shift, (m_s, acc_s), (m_in, acc_in), out_ref)
         part = jnp.concatenate(stats, axis=0)
         rows = jnp.concatenate([*thirds(part), jnp.zeros((META - 12, 128), F32)], axis=0)
         out_ref[BLOCK:, :] = rows.astype(BF)
@@ -319,18 +314,18 @@
 
 def merge(i, t, shift, front, back, out_ref):
     (m_s, acc_s), (bm, bacc) = front, back
-    best_f = m_s[i, :1, :]
-    best_b = jnp.where(bacc[i, 128:129, :] > 0.0, bm[i, :1, :] + shift, NEG)
+    best_f = m_s[FRONT, i, :1, :]
+    best_b = jnp.where(bacc[BACK, i, 128:129, :] > 0.0, bm[BACK, i, :1, :] + shift, NEG)
     best = jnp.maximum(best_f, best_b)
     safe = jnp.where(best < -1e29, 0.0, best)
     wf = jnp.exp(best_f - safe)
     wb = jnp.exp(best_b - safe)
-    total = wf * acc_s[i, 128:129, :] + wb * bacc[i, 128:129, :]
+    total = wf * acc_s[FRONT, i, 128:129, :] + wb * bacc[BACK, i, 128:129, :]
     some = total > 0.0
     total = jnp.where(some, total, 1.0)
     wf = wf / total
     wb = wb / total
-    mix = wf * acc_s[i, :128, :] + wb * bacc[i, :128, :]
+    mix = wf * acc_s[FRONT, i, :128, :] + wb * bacc[BACK, i, :128, :]
     lse = jnp.where(some, best + jnp.log(total), NEG)
     stats = []
     for g in range(QT // 128):
@@ -388,9 +383,9 @@
 
 
 STATE = (
-    shape(8, 128, dtype=F32),
-    shape(TILES, 8, QT, dtype=F32),
-    shape(TILES, ACC, QT, dtype=F32),
+    shape(2, 8, 128, dtype=F32),
+    shape(2, TILES, 8, QT, dtype=F32),
+    shape(2, TILES, ACC, QT, dtype=F32),
 )
 LOADED = [VMEM((KEYS, 256), BF), VMEM((ACC, KEYS), BF)]
 
@@ -450,23 +445,20 @@
     far0 = hop(kf[3][:2], 1)
     far1 = hop(kb[3][2:], -1)
 
-    qa, *front = attention(diag_kernel, (shape(SLAB, 256), *STATE), 6)(ids, *qs, kv)
-    back = []
+    qa, *state = attention(diag_kernel, (shape(SLAB, 256), *STATE), 6)(ids, *qs, kv)
     for s in range(1, 4):
-        back = attention(
-            functools.partial(back_kernel, s), STATE, 3 + len(back),
-            {3: 0, 4: 1, 5: 2} if back else None,
-        )(ids, qa, kb[s], *back)
-        front = attention(
-            functools.partial(front_kernel, s), STATE, 6, {3: 0, 4: 1, 5: 2}
-        )(ids, qa, kf[s], *front)
+        state = attention(
+            functools.partial(step_kernel, s), STATE, 7, {4: 0, 5: 1, 6: 2}
+        )(ids, qa, kb[s], kf[s], *state)
     outs = attention(
-        last_kernel, (shape(BLOCK + META, 128),) * NX, 10, None, [VMEM(s.shape, F32) for s in STATE]
-    )(ids, qa, far0, far1, *front, *back)
+        last_kernel,
+        (shape(BLOCK + META, 128),) * NX,
+        7,
+        None,
+        [VMEM((8, 128), F32), *(VMEM(s.shape, F32) for s in STATE[1:])],
+    )(ids, qa, far0, far1, *state)
     parts = swap(outs)
-    att = call(
-        join_kernel, shape(NY * NC, PIECE, COLS), [sspec()] + [vspec()] * 5, 1 << 20
-    )(ids, *parts, gate)
+    att = call(join_kernel, shape(NY * NC, PIECE, COLS), [sspec()] + [vspec()] * 5, 1 << 20)(ids, *parts, gate)
     rows = lax.all_to_all(att, ("y", "c"), 0, 0, tiled=True)
     return call(
         out_kernel, shape(PIECE, WIDTH), [vspec()] * 2, 2 * PIECE * WIDTH * WIDTH,

time: 148 us -> 140 us (0.946)
  Pallas kernels: 50.9 us -> 44.6 us
    pallas_call x7 -> x4, Pallas kernels: 30.7 us -> 24.7 us  [the longest x3 20.4 us: body(): attention(functools.partial(step_kernel, s), STATE, 7, {4: 0, 5: 1, 6: 2})]
  transfers between devices with their start and end apart: 21 -> 21, of which waited for: 10 -> 10; matrix products, arithmetic and copies ran while one was open for 0% -> 0% of each run, Pallas kernels for 25% -> 23%
where the time goes in v2:
time: 140 us
  Pallas kernels  44.6 us (32%)
  waiting for transfers between devices  38.6 us (28%)
  blocking collectives  25 us (18%)
  starting transfers between devices  24.8 us (18%)
  local copies, waits for them, and re-layouts  6.08 us (4%)
    ppermute x8, waiting for transfers between devices, hop(): return lax.ppermute(value, 'z', ring(NZ, direction))  21.6 us
    pallas_call x3, Pallas kernels, body(): attention(functools.partial(step_kernel, s), STATE, 7, {4: 0, 5: 1, 6: 2})  20.4 us
    all_to_all x1, blocking collectives, body(): kv = lax.all_to_all(kvx, 'x', 0, 0, tiled=True)  14.3 us
    pallas_call x3, Pallas kernels, project(): call(kernel, outs, [sspec()] + [hbm] * (8 + len(weights)) + list(specs),...  13.9 us
    all_to_all x1, blocking collectives, body(): rows = lax.all_to_all(att, ('y', 'c'), 0, 0, tiled=True)  10.8 us
    ppermute x8, starting transfers between devices, hop(): return lax.ppermute(value, 'z', ring(NZ, direction))  10.5 us
    ppermute x3, waiting for transfers between devices, body(): lax.ppermute(tokens, 'y', ring(NY, s))  10.5 us
    ppermute x6, starting transfers between devices, swap(): out.append(lax.ppermute(values[s], 'x', ring(NX, s)))  7.97 us
  transfers between devices with their start and end apart: 21, of which 10 were waited for; matrix products, arithmetic and copies ran while one was open for 0% of the time, Pallas kernels for 23%

profile of v2, /device:TPU:224, one launch (start us, length us, event | category | flops | bytes accessed | tf_op | source)
XLA Modules:
  0.0 140.0 jit_solution(14571415044376581938)
XLA Ops:
  0.0 1.6 %collective-permute-start = (bf16[64,2048]{1,0:T(8,128)(2,1)}, bf16[64,2048]{1,0:T(8,128)(2,1)S(1)}, u32[]{:S(2)}, u32[]{:S(2)}) collective-permute-start(bf16[64,2048]{1,0:T(8,128)(2,1)} %refs_0_.5), channel_id=1, source_target_pairs={{0,2},{2,4},{4,6},{6,0},{1,3},{3,5},{5,7},{7,1},{8,10},{10,12},{12... | collective-permute-start | bytes 786440 | tf_op jit(solution)/shard_map/ppermute | solution.py:406
  1.6 2.9 %collective-permute-start.1 = (bf16[64,2048]{1,0:T(8,128)(2,1)}, bf16[64,2048]{1,0:T(8,128)(2,1)S(1)}, u32[]{:S(2)}, u32[]{:S(2)}) collective-permute-start(bf16[64,2048]{1,0:T(8,128)(2,1)} %refs_0_.5), channel_id=1, source_target_pairs={{0,4},{2,6},{4,0},{6,2},{1,5},{3,7},{5,1},{7,3},{8,12},{10,14},{12... | collective-permute-start | bytes 786440 | tf_op jit(solution)/shard_map/ppermute | solution.py:406
  4.5 1.3 collective-permute-start.2
  5.8 3.7 %collective-permute-done.refs_1_ = bf16[64,2048]{1,0:T(8,128)(2,1)S(1)} collective-permute-done((bf16[64,2048]{1,0:T(8,128)(2,1)}, bf16[64,2048]{1,0:T(8,128)(2,1)S(1)}, u32[]{:S(2)}, u32[]{:S(2)}) %collective-permute-start) | collective-permute-done | bytes 262176 | tf_op jit(solution)/shard_map/ppermute | solution.py:406
  9.5 6.8 %collective-permute-done.1.refs_2_ = bf16[64,2048]{1,0:T(8,128)(2,1)S(1)} collective-permute-done((bf16[64,2048]{1,0:T(8,128)(2,1)}, bf16[64,2048]{1,0:T(8,128)(2,1)S(1)}, u32[]{:S(2)}, u32[]{:S(2)}) %collective-permute-start.1) | collective-permute-done | bytes 262176 | tf_op jit(solution)/shard_map/ppermute | solution.py:406
  18.9 5.7 %shard_map.83 = bf16[4,528,128]{2,1,0:T(8,128)(2,1)} custom-call(s32[4]{0:T(128)} %pad_add_fusion.ids_ref, bf16[64,2048]{1,0:T(8,128)(2,1)} %refs_0_.5, bf16[64,2048]{1,0:T(8,128)(2,1)} %copy-done.5, bf16[64,2048]{1,0:T(8,128)(2,1)} %copy-done.6, bf16[64,2048]{1,0:T(8,128)(2,1)} %copy-done.7, bf16[64,2048]{1,0:T(8,128)(2,1)} %copy-done.8, ...), custom_call_target="tpu_custom_call" | custom-call | flops 1073741824 | bytes 2097152 | tf_op jit(solution)/shard_map/pallas_call | solution.py:414
  24.7 14.3 %all_to_all.10.kv_ref = bf16[4,528,128]{2,1,0:T(8,128)(2,1)S(1)} all-to-all(bf16[4,528,128]{2,1,0:T(8,128)(2,1)} %shard_map.83), channel_id=1, replica_groups=mesh['z'=8,'x'=4,'y'=4,'c'=2] {'x'}, dimensions={0} | all-to-all | bytes 1081344 | tf_op jit(solution)/shard_map/all_to_all | solution.py:426
  38.9 2.0 %collective-permute-start.14 = (bf16[4,528,128]{2,1,0:T(8,128)(2,1)S(1)}, bf16[4,528,128]{2,1,0:T(8,128)(2,1)S(1)}, u32[]{:S(2)}, u32[]{:S(2)}) collective-permute-start(bf16[4,528,128]{2,1,0:T(8,128)(2,1)S(1)} %all_to_all.10.kv_ref), channel_id=1, source_target_pairs={{0,224},{32,0},{64,32},{96,64},{128,96},{160,128},{192,160},{224,1... | collective-permute-start | bytes 1622024 | tf_op jit(solution)/shard_map/ppermute | solution.py:439
  40.9 11.2 %collective-permute-done.10.front_ref = bf16[4,528,128]{2,1,0:T(8,128)(2,1)S(1)} collective-permute-done((bf16[4,528,128]{2,1,0:T(8,128)(2,1)S(1)}, bf16[4,528,128]{2,1,0:T(8,128)(2,1)S(1)}, u32[]{:S(2)}, u32[]{:S(2)}) %collective-permute-start.10) | collective-permute-done | bytes 540704 | tf_op jit(solution)/shard_map/ppermute | solution.py:439
  52.1 1.5 %collective-permute-start.11 = (bf16[4,528,128]{2,1,0:T(8,128)(2,1)S(1)}, bf16[4,528,128]{2,1,0:T(8,128)(2,1)S(1)}, u32[]{:S(2)}, u32[]{:S(2)}) collective-permute-start(bf16[4,528,128]{2,1,0:T(8,128)(2,1)S(1)} %collective-permute-done.10.front_ref), channel_id=1, source_target_pairs={{0,32},{32,64},{64,96},{96,128},{128,160},{160,192},{192,224},{224... | collective-permute-start | bytes 1622024 | tf_op jit(solution)/shard_map/ppermute | solution.py:439
  54.1 10.4 %collective-permute-done.11.front_ref = bf16[4,528,128]{2,1,0:T(8,128)(2,1)S(1)} collective-permute-done((bf16[4,528,128]{2,1,0:T(8,128)(2,1)S(1)}, bf16[4,528,128]{2,1,0:T(8,128)(2,1)S(1)}, u32[]{:S(2)}, u32[]{:S(2)}) %collective-permute-start.11) | collective-permute-done | bytes 540704 | tf_op jit(solution)/shard_map/ppermute | solution.py:439
  64.5 2.9 %collective-permute-start.12 = (bf16[4,528,128]{2,1,0:T(8,128)(2,1)S(1)}, bf16[4,528,128]{2,1,0:T(8,128)(2,1)S(1)}, u32[]{:S(2)}, u32[]{:S(2)}) collective-permute-start(bf16[4,528,128]{2,1,0:T(8,128)(2,1)S(1)} %collective-permute-done.11.front_ref), channel_id=1, source_target_pairs={{0,32},{32,64},{64,96},{96,128},{128,160},{160,192},{192,224},{224... | collective-permute-start | bytes 1622024 | tf_op jit(solution)/shard_map/ppermute | solution.py:439
  67.4 4.1 %shard_map.82 = (bf16[512,128]{1,0:T(8,128)(2,1)}, bf16[512,128]{1,0:T(8,128)(2,1)}) custom-call(s32[4]{0:T(128)} %pad_add_fusion.ids_ref, bf16[64,2048]{1,0:T(8,128)(2,1)} %refs_0_.5, bf16[64,2048]{1,0:T(8,128)(2,1)} %copy-done.5, bf16[64,2048]{1,0:T(8,128)(2,1)} %copy-done.6, bf16[64,2048]{1,0:T(8,128)(2,1)} %copy-done.7, bf16[64,2048]{1,0:T(8,128)(2,1)} %copy-done.8, ...), custom_call_target="tpu_custom_call" | custom-call | flops 536870912 | bytes 2097152 | tf_op jit(solution)/shard_map/pallas_call | solution.py:414
  72.1 2.1 %collective-permute-start.8 = (bf16[512,128]{1,0:T(8,128)(2,1)}, bf16[512,128]{1,0:T(8,128)(2,1)S(1)}, u32[]{:S(2)}, u32[]{:S(2)}) collective-permute-start(bf16[512,128]{1,0:T(8,128)(2,1)} %get-tuple-element.24.q0), channel_id=1, source_target_pairs={{0,16},{8,24},{16,0},{24,8},{1,17},{9,25},{17,1},{25,9},{2,18},{10... | collective-permute-start | bytes 393224 | tf_op jit(solution)/shard_map/ppermute | solution.py:432
  74.2 1.0 collective-permute-start.9
  75.2 4.1 %collective-permute-done.7.q1 = bf16[512,128]{1,0:T(8,128)(2,1)S(1)} collective-permute-done((bf16[512,128]{1,0:T(8,128)(2,1)}, bf16[512,128]{1,0:T(8,128)(2,1)S(1)}, u32[]{:S(2)}, u32[]{:S(2)}) %collective-permute-start.7) | collective-permute-done | bytes 131104 | tf_op jit(solution)/shard_map/ppermute | solution.py:432
  79.4 0.9 collective-permute-done.9.q3
  80.2 0.9 copy-done.4
  81.1 3.0 %shard_map.84 = (bf16[2048,256]{1,0:T(8,128)(2,1)S(1)}, f32[2,8,128]{2,1,0:T(8,128)S(1)}, f32[2,4,8,512]{3,2,1,0:T(8,128)S(1)}, f32[2,4,144,512]{3,2,1,0:T(8,128)S(1)}) custom-call(s32[4]{0:T(128)S(1)} %copy-done.2, bf16[512,128]{1,0:T(8,128)(2,1)S(1)} %copy-done.4, bf16[512,128]{1,0:T(8,128)(2,1)S(1)} %collective-permute-done.7.q1, ...), custom_call_target="tpu_custom_call" | custom-call | flops 1073741824 | bytes 2097152 | tf_op jit(solution)/shard_map/pallas_call | solution.py:448
  84.1 3.3 %collective-permute-start.13 = (bf16[2,528,128]{2,1,0:T(8,128)(2,1)S(1)}, bf16[2,528,128]{2,1,0:T(8,128)(2,1)S(1)}, u32[]{:S(2)}, u32[]{:S(2)}) collective-permute-start(bf16[2,528,128]{2,1,0:T(8,128)(2,1)S(1)} %slice.8), channel_id=1, source_target_pairs={{0,32},{32,64},{64,96},{96,128},{128,160},{160,192},{192,224},{224... | collective-permute-start | bytes 811016 | tf_op jit(solution)/shard_map/ppermute | solution.py:439
  87.8 6.8 %shard_map.85 = (f32[2,8,128]{2,1,0:T(8,128)S(1)}, f32[2,4,8,512]{3,2,1,0:T(8,128)S(1)}, f32[2,4,144,512]{3,2,1,0:T(8,128)S(1)}) custom-call(s32[4]{0:T(128)S(1)} %copy-done.2, bf16[2048,256]{1,0:T(8,128)(2,1)S(1)} %get-tuple-element.26.qa_ref, ...), custom_call_target="tpu_custom_call", output_to_operand_aliasing={{0}: (4, {}), {1}: (5, {}), {2}: (6, {})} | custom-call | flops 1073741824 | bytes 2097152 | tf_op jit(solution)/shard_map/pallas_call | solution.py:450
  94.6 6.8 %shard_map.86 = (f32[2,8,128]{2,1,0:T(8,128)S(1)}, f32[2,4,8,512]{3,2,1,0:T(8,128)S(1)}, f32[2,4,144,512]{3,2,1,0:T(8,128)S(1)}) custom-call(s32[4]{0:T(128)S(1)} %copy-done.2, bf16[2048,256]{1,0:T(8,128)(2,1)S(1)} %get-tuple-element.26.qa_ref, ...), custom_call_target="tpu_custom_call", output_to_operand_aliasing={{0}: (4, {}), {1}: (5, {}), {2}: (6, {})} | custom-call | flops 1073741824 | bytes 2097152 | tf_op jit(solution)/shard_map/pallas_call | solution.py:450
  101.4 6.8 %shard_map.87 = (f32[2,8,128]{2,1,0:T(8,128)S(1)}, f32[2,4,8,512]{3,2,1,0:T(8,128)S(1)}, f32[2,4,144,512]{3,2,1,0:T(8,128)S(1)}) custom-call(s32[4]{0:T(128)S(1)} %copy-done.2, bf16[2048,256]{1,0:T(8,128)(2,1)S(1)} %get-tuple-element.26.qa_ref, ...), custom_call_target="tpu_custom_call", output_to_operand_aliasing={{0}: (4, {}), {1}: (5, {}), {2}: (6, {})} | custom-call | flops 1073741824 | bytes 2097152 | tf_op jit(solution)/shard_map/pallas_call | solution.py:450
  108.3 4.3 %shard_map.88 = (bf16[528,128]{1,0:T(8,128)(2,1)S(1)}, bf16[528,128]{1,0:T(8,128)(2,1)S(1)}, bf16[528,128]{1,0:T(8,128)(2,1)S(1)}, bf16[528,128]{1,0:T(8,128)(2,1)S(1)}) custom-call(s32[4]{0:T(128)S(1)} %copy-done.2, bf16[2048,256]{1,0:T(8,128)(2,1)S(1)} %get-tuple-element.26.qa_ref, bf16[2,528,128]{2,1,0:T(8,128)(2,1)S(1)} %collective-permute-done.13.kv0_ref, ...), custom_call_target="tpu_custom_call" | custom-call | flops 1073741824 | bytes 2097152 | tf_op jit(solution)/shard_map/pallas_call | solution.py:453
  112.5 0.7 collective-permute-start.18
  113.3 3.5 %collective-permute-start.19 = (bf16[528,128]{1,0:T(8,128)(2,1)S(1)}, bf16[528,128]{1,0:T(8,128)(2,1)S(1)}, u32[]{:S(2)}, u32[]{:S(2)}) collective-permute-start(bf16[528,128]{1,0:T(8,128)(2,1)S(1)} %get-tuple-element.41), channel_id=1, source_target_pairs={{0,16},{8,24},{16,0},{24,8},{1,17},{9,25},{17,1},{25,9},{2,18},{10... | collective-permute-start | bytes 405512 | tf_op jit(solution)/shard_map/ppermute | solution.py:432
  116.8 4.2 %shard_map.89.gate_ref = f32[2,512,128]{2,1,0:T(8,128)} custom-call(s32[4]{0:T(128)} %pad_add_fusion.ids_ref, bf16[64,2048]{1,0:T(8,128)(2,1)} %refs_0_.5, bf16[64,2048]{1,0:T(8,128)(2,1)} %copy-done.5, bf16[64,2048]{1,0:T(8,128)(2,1)} %copy-done.6, bf16[64,2048]{1,0:T(8,128)(2,1)} %copy-done.7, bf16[64,2048]{1,0:T(8,128)(2,1)} %copy-done.8, ...), custom_call_target="tpu_custom_call" | custom-call | flops 536870912 | bytes 2097152 | tf_op jit(solution)/shard_map/pallas_call | solution.py:414
  121.8 1.0 copy-done.1
  122.8 0.8 shard_map.90
  123.6 10.8 %all_to_all.11.rows_ref = bf16[8,64,256]{2,1,0:T(8,128)(2,1)S(1)} all-to-all(bf16[8,64,256]{2,1,0:T(8,128)(2,1)S(1)} %shard_map.90), channel_id=1, replica_groups=mesh['z'=8,'x'=4,'y'=4,'c'=2] {'y','c'}, dimensions={0} | all-to-all | bytes 524288 | tf_op jit(solution)/shard_map/all_to_all | solution.py:462
  134.4 3.4 %copy-done = bf16[2048,2048]{1,0:T(8,128)(2,1)S(1)} copy-done((bf16[2048,2048]{1,0:T(8,128)(2,1)S(1)}, bf16[2048,2048]{1,0:T(8,128)(2,1)}, u32[]{:S(2)}) %copy-start) | copy-done | bytes 8388632
  137.8 2.3 %shard_map.91 = bf16[64,2048]{1,0:T(8,128)(2,1)} custom-call(bf16[8,64,256]{2,1,0:T(8,128)(2,1)S(1)} %all_to_all.11.rows_ref, bf16[2048,2048]{1,0:T(8,128)(2,1)S(1)} %copy-done), custom_call_target="tpu_custom_call" | custom-call | flops 536870912 | bytes 2097152 | tf_op jit(solution)/shard_map/pallas_call | solution.py:463
  (49 shorter events, 5.0 us)
Async XLA Ops:
  0.0 9.5 %collective-permute-start = (bf16[64,2048]{1,0:T(8,128)(2,1)}, bf16[64,2048]{1,0:T(8,128)(2,1)S(1)}, u32[]{:S(2)}, u32[]{:S(2)}) collective-permute-start(bf16[64,2048]{1,0:T(8,128)(2,1)} %refs_0_.5), channel_id=1, source_target_pairs={{0,2},{2,4},{4,6},{6,0},{1,3},{3,5},{5,7},{7,1},{8,10},{10,12},{12... | collective-permute-start | bytes 786440 | tf_op jit(solution)/shard_map/ppermute | solution.py:406
  1.6 14.7 %collective-permute-start.1 = (bf16[64,2048]{1,0:T(8,128)(2,1)}, bf16[64,2048]{1,0:T(8,128)(2,1)S(1)}, u32[]{:S(2)}, u32[]{:S(2)}) collective-permute-start(bf16[64,2048]{1,0:T(8,128)(2,1)} %refs_0_.5), channel_id=1, source_target_pairs={{0,4},{2,6},{4,0},{6,2},{1,5},{3,7},{5,1},{7,3},{8,12},{10,14},{12... | collective-permute-start | bytes 786440 | tf_op jit(solution)/shard_map/ppermute | solution.py:406
  4.5 11.9 %collective-permute-start.2 = (bf16[64,2048]{1,0:T(8,128)(2,1)}, bf16[64,2048]{1,0:T(8,128)(2,1)S(1)}, u32[]{:S(2)}, u32[]{:S(2)}) collective-permute-start(bf16[64,2048]{1,0:T(8,128)(2,1)} %refs_0_.5), channel_id=1, source_target_pairs={{0,6},{2,0},{4,2},{6,4},{1,7},{3,1},{5,3},{7,5},{8,14},{10,8},{12,... | collective-permute-start | bytes 786440 | tf_op jit(solution)/shard_map/ppermute | solution.py:406
  5.8 11.7 %collective-permute-start.3 = (bf16[64,2048]{1,0:T(8,128)(2,1)}, bf16[64,2048]{1,0:T(8,128)(2,1)S(1)}, u32[]{:S(2)}, u32[]{:S(2)}) collective-permute-start(bf16[64,2048]{1,0:T(8,128)(2,1)} %refs_0_.5), channel_id=1, source_target_pairs={{0,1},{1,0},{2,3},{3,2},{4,5},{5,4},{6,7},{7,6},{8,9},{9,8},{10,11... | collective-permute-start | bytes 786440 | tf_op jit(solution)/shard_map/ppermute | solution.py:407
  9.5 8.7 %copy-start.5 = (bf16[64,2048]{1,0:T(8,128)(2,1)}, bf16[64,2048]{1,0:T(8,128)(2,1)S(1)}, u32[]{:S(2)}) copy-start(bf16[64,2048]{1,0:T(8,128)(2,1)S(1)} %collective-permute-done.refs_1_) | copy-start | bytes 786436
  9.5 8.0 %collective-permute-start.4 = (bf16[64,2048]{1,0:T(8,128)(2,1)S(1)}, bf16[64,2048]{1,0:T(8,128)(2,1)S(1)}, u32[]{:S(2)}, u32[]{:S(2)}) collective-permute-start(bf16[64,2048]{1,0:T(8,128)(2,1)S(1)} %collective-permute-done.refs_1_), channel_id=1, source_target_pairs={{0,1},{1,0},{2,3},{3,2},{4,5},{5,4},{6,7},{7,6},{8,9},{9,8},{10,11... | collective-permute-start | bytes 786440 | tf_op jit(solution)/shard_map/ppermute | solution.py:408
  16.3 1.9 %copy-start.6 = (bf16[64,2048]{1,0:T(8,128)(2,1)}, bf16[64,2048]{1,0:T(8,128)(2,1)S(1)}, u32[]{:S(2)}) copy-start(bf16[64,2048]{1,0:T(8,128)(2,1)S(1)} %collective-permute-done.1.refs_2_) | copy-start | bytes 786436
  16.3 1.5 %collective-permute-start.5 = (bf16[64,2048]{1,0:T(8,128)(2,1)S(1)}, bf16[64,2048]{1,0:T(8,128)(2,1)S(1)}, u32[]{:S(2)}, u32[]{:S(2)}) collective-permute-start(bf16[64,2048]{1,0:T(8,128)(2,1)S(1)} %collective-permute-done.1.refs_2_), channel_id=1, source_target_pairs={{0,1},{1,0},{2,3},{3,2},{4,5},{5,4},{6,7},{7,6},{8,9},{9,8},{10,11... | collective-permute-start | bytes 786440 | tf_op jit(solution)/shard_map/ppermute | solution.py:408
  16.3 1.9 %copy-start.7 = (bf16[64,2048]{1,0:T(8,128)(2,1)}, bf16[64,2048]{1,0:T(8,128)(2,1)S(1)}, u32[]{:S(2)}) copy-start(bf16[64,2048]{1,0:T(8,128)(2,1)S(1)} %collective-permute-done.2.refs_3_) | copy-start | bytes 786436
  16.3 1.9 %collective-permute-start.6 = (bf16[64,2048]{1,0:T(8,128)(2,1)S(1)}, bf16[64,2048]{1,0:T(8,128)(2,1)S(1)}, u32[]{:S(2)}, u32[]{:S(2)}) collective-permute-start(bf16[64,2048]{1,0:T(8,128)(2,1)S(1)} %collective-permute-done.2.refs_3_), channel_id=1, source_target_pairs={{0,1},{1,0},{2,3},{3,2},{4,5},{5,4},{6,7},{7,6},{8,9},{9,8},{10,11... | collective-permute-start | bytes 786440 | tf_op jit(solution)/shard_map/ppermute | solution.py:408
  17.5 0.8 copy-start.8
  17.5 0.8 copy-start.9
  18.2 0.7 copy-start.11
  24.6 55.6 %copy-start.2 = (s32[4]{0:T(128)S(1)}, s32[4]{0:T(128)}, u32[]{:S(2)}) copy-start(s32[4]{0:T(128)} %pad_add_fusion.ids_ref) | copy-start | bytes 52
  38.9 13.2 %collective-permute-start.10 = (bf16[4,528,128]{2,1,0:T(8,128)(2,1)S(1)}, bf16[4,528,128]{2,1,0:T(8,128)(2,1)S(1)}, u32[]{:S(2)}, u32[]{:S(2)}) collective-permute-start(bf16[4,528,128]{2,1,0:T(8,128)(2,1)S(1)} %all_to_all.10.kv_ref), channel_id=1, source_target_pairs={{0,32},{32,64},{64,96},{96,128},{128,160},{160,192},{192,224},{224... | collective-permute-start | bytes 1622024 | tf_op jit(solution)/shard_map/ppermute | solution.py:439
  38.9 14.7 %collective-permute-start.14 = (bf16[4,528,128]{2,1,0:T(8,128)(2,1)S(1)}, bf16[4,528,128]{2,1,0:T(8,128)(2,1)S(1)}, u32[]{:S(2)}, u32[]{:S(2)}) collective-permute-start(bf16[4,528,128]{2,1,0:T(8,128)(2,1)S(1)} %all_to_all.10.kv_ref), channel_id=1, source_target_pairs={{0,224},{32,0},{64,32},{96,64},{128,96},{160,128},{192,160},{224,1... | collective-permute-start | bytes 1622024 | tf_op jit(solution)/shard_map/ppermute | solution.py:439
  52.1 12.4 %collective-permute-start.11 = (bf16[4,528,128]{2,1,0:T(8,128)(2,1)S(1)}, bf16[4,528,128]{2,1,0:T(8,128)(2,1)S(1)}, u32[]{:S(2)}, u32[]{:S(2)}) collective-permute-start(bf16[4,528,128]{2,1,0:T(8,128)(2,1)S(1)} %collective-permute-done.10.front_ref), channel_id=1, source_target_pairs={{0,32},{32,64},{64,96},{96,128},{128,160},{160,192},{192,224},{224... | collective-permute-start | bytes 1622024 | tf_op jit(solution)/shard_map/ppermute | solution.py:439
  53.6 13.8 %collective-permute-start.15 = (bf16[4,528,128]{2,1,0:T(8,128)(2,1)S(1)}, bf16[4,528,128]{2,1,0:T(8,128)(2,1)S(1)}, u32[]{:S(2)}, u32[]{:S(2)}) collective-permute-start(bf16[4,528,128]{2,1,0:T(8,128)(2,1)S(1)} %collective-permute-done.14.back_ref), channel_id=1, source_target_pairs={{0,224},{32,0},{64,32},{96,64},{128,96},{160,128},{192,160},{224,1... | collective-permute-start | bytes 1622024 | tf_op jit(solution)/shard_map/ppermute | solution.py:439
  64.5 19.6 %collective-permute-start.12 = (bf16[4,528,128]{2,1,0:T(8,128)(2,1)S(1)}, bf16[4,528,128]{2,1,0:T(8,128)(2,1)S(1)}, u32[]{:S(2)}, u32[]{:S(2)}) collective-permute-start(bf16[4,528,128]{2,1,0:T(8,128)(2,1)S(1)} %collective-permute-done.11.front_ref), channel_id=1, source_target_pairs={{0,32},{32,64},{64,96},{96,128},{128,160},{160,192},{192,224},{224... | collective-permute-start | bytes 1622024 | tf_op jit(solution)/shard_map/ppermute | solution.py:439
  67.4 20.0 %collective-permute-start.16 = (bf16[4,528,128]{2,1,0:T(8,128)(2,1)S(1)}, bf16[4,528,128]{2,1,0:T(8,128)(2,1)S(1)}, u32[]{:S(2)}, u32[]{:S(2)}) collective-permute-start(bf16[4,528,128]{2,1,0:T(8,128)(2,1)S(1)} %collective-permute-done.15.back_ref), channel_id=1, source_target_pairs={{0,224},{32,0},{64,32},{96,64},{128,96},{160,128},{192,160},{224,1... | collective-permute-start | bytes 1622024 | tf_op jit(solution)/shard_map/ppermute | solution.py:439
  71.5 7.9 %collective-permute-start.7 = (bf16[512,128]{1,0:T(8,128)(2,1)}, bf16[512,128]{1,0:T(8,128)(2,1)S(1)}, u32[]{:S(2)}, u32[]{:S(2)}) collective-permute-start(bf16[512,128]{1,0:T(8,128)(2,1)} %get-tuple-element.25), channel_id=1, source_target_pairs={{0,8},{8,16},{16,24},{24,0},{1,9},{9,17},{17,25},{25,1},{2,10},{10... | collective-permute-start | bytes 393224 | tf_op jit(solution)/shard_map/ppermute | solution.py:432
  72.1 7.2 %collective-permute-start.8 = (bf16[512,128]{1,0:T(8,128)(2,1)}, bf16[512,128]{1,0:T(8,128)(2,1)S(1)}, u32[]{:S(2)}, u32[]{:S(2)}) collective-permute-start(bf16[512,128]{1,0:T(8,128)(2,1)} %get-tuple-element.24.q0), channel_id=1, source_target_pairs={{0,16},{8,24},{16,0},{24,8},{1,17},{9,25},{17,1},{25,9},{2,18},{10... | collective-permute-start | bytes 393224 | tf_op jit(solution)/shard_map/ppermute | solution.py:432
  74.2 6.0 %collective-permute-start.9 = (bf16[512,128]{1,0:T(8,128)(2,1)}, bf16[512,128]{1,0:T(8,128)(2,1)S(1)}, u32[]{:S(2)}, u32[]{:S(2)}) collective-permute-start(bf16[512,128]{1,0:T(8,128)(2,1)} %get-tuple-element.25), channel_id=1, source_target_pairs={{0,24},{8,0},{16,8},{24,16},{1,25},{9,1},{17,9},{25,17},{2,26},{10... | collective-permute-start | bytes 393224 | tf_op jit(solution)/shard_map/ppermute | solution.py:432
  80.2 0.9 copy-start.4
  84.1 24.1 %collective-permute-start.13 = (bf16[2,528,128]{2,1,0:T(8,128)(2,1)S(1)}, bf16[2,528,128]{2,1,0:T(8,128)(2,1)S(1)}, u32[]{:S(2)}, u32[]{:S(2)}) collective-permute-start(bf16[2,528,128]{2,1,0:T(8,128)(2,1)S(1)} %slice.8), channel_id=1, source_target_pairs={{0,32},{32,64},{64,96},{96,128},{128,160},{160,192},{192,224},{224... | collective-permute-start | bytes 811016 | tf_op jit(solution)/shard_map/ppermute | solution.py:439
  87.5 20.8 %collective-permute-start.17 = (bf16[2,528,128]{2,1,0:T(8,128)(2,1)S(1)}, bf16[2,528,128]{2,1,0:T(8,128)(2,1)S(1)}, u32[]{:S(2)}, u32[]{:S(2)}) collective-permute-start(bf16[2,528,128]{2,1,0:T(8,128)(2,1)S(1)} %slice.9), channel_id=1, source_target_pairs={{0,224},{32,0},{64,32},{96,64},{128,96},{160,128},{192,160},{224,1... | collective-permute-start | bytes 811016 | tf_op jit(solution)/shard_map/ppermute | solution.py:439
  112.5 9.2 %copy-start.3 = (s32[4]{0:T(128)S(1)}, s32[4]{0:T(128)}, u32[]{:S(2)}) copy-start(s32[4]{0:T(128)} %pad_add_fusion.ids_ref) | copy-start | bytes 52
  112.5 8.4 %collective-permute-start.18 = (bf16[528,128]{1,0:T(8,128)(2,1)S(1)}, bf16[528,128]{1,0:T(8,128)(2,1)S(1)}, u32[]{:S(2)}, u32[]{:S(2)}) collective-permute-start(bf16[528,128]{1,0:T(8,128)(2,1)S(1)} %get-tuple-element.40), channel_id=1, source_target_pairs={{0,8},{8,16},{16,24},{24,0},{1,9},{9,17},{17,25},{25,1},{2,10},{10... | collective-permute-start | bytes 405512 | tf_op jit(solution)/shard_map/ppermute | solution.py:432
  113.3 7.9 %collective-permute-start.19 = (bf16[528,128]{1,0:T(8,128)(2,1)S(1)}, bf16[528,128]{1,0:T(8,128)(2,1)S(1)}, u32[]{:S(2)}, u32[]{:S(2)}) collective-permute-start(bf16[528,128]{1,0:T(8,128)(2,1)S(1)} %get-tuple-element.41), channel_id=1, source_target_pairs={{0,16},{8,24},{16,0},{24,8},{1,17},{9,25},{17,1},{25,9},{2,18},{10... | collective-permute-start | bytes 405512 | tf_op jit(solution)/shard_map/ppermute | solution.py:432
  116.8 5.0 %collective-permute-start.20 = (bf16[528,128]{1,0:T(8,128)(2,1)S(1)}, bf16[528,128]{1,0:T(8,128)(2,1)S(1)}, u32[]{:S(2)}, u32[]{:S(2)}) collective-permute-start(bf16[528,128]{1,0:T(8,128)(2,1)S(1)} %get-tuple-element.42), channel_id=1, source_target_pairs={{0,24},{8,0},{16,8},{24,16},{1,25},{9,1},{17,9},{25,17},{2,26},{10... | collective-permute-start | bytes 405512 | tf_op jit(solution)/shard_map/ppermute | solution.py:432
  121.8 1.0 copy-start.1
  134.4 3.4 %copy-start = (bf16[2048,2048]{1,0:T(8,128)(2,1)S(1)}, bf16[2048,2048]{1,0:T(8,128)(2,1)}, u32[]{:S(2)}) copy-start(bf16[2048,2048]{1,0:T(8,128)(2,1)} %wo_ref.1) | copy-start | bytes 25165828
  (1 other events, 0.7 us)

commit v3 on v2

--- a/solution.py
+++ b/solution.py
@@ -15,6 +15,7 @@
 HALF = 256
 SLAB = NX * BLOCK
 PIECE = 64
+PIECES = 10
 WIDTH = 2048
 COLS = 256
 META = 16
@@ -46,10 +47,11 @@
 def fetch(ids_ref, pieces, toks_ref, weights, sems):
     y, c = ids_ref[2], ids_ref[3]
     pairs = []
-    for i in range(8):
-        pos = 2 * ((y + NY - i % NY) % NY) + (c if i < NY else 1 - c)
-        start = pl.multiple_of(pos * PIECE, PIECE)
-        pairs.append((pieces[i], toks_ref.at[pl.ds(start, PIECE), :]))
+    for i, piece in enumerate(pieces):
+        away, offset = ((0, 0), (1, 0), (3, 0), (2, 0), (2, PIECE // 2))[i % 5]
+        pos = 2 * ((y + NY - away) % NY) + (c if i < 5 else 1 - c)
+        start = pl.multiple_of(pos * PIECE + offset, PIECE // 2)
+        pairs.append((piece, toks_ref.at[pl.ds(start, piece.shape[0]), :]))
     parts = 4
     for source, target in weights:
         for i in range(parts):
@@ -61,7 +63,7 @@
     ]
     for copy in copies:
         copy.start()
-    return copies[:8], copies[8:]
+    return copies[: len(pieces)], copies[len(pieces) :]
 
 
 def wait_all(copies):
@@ -70,10 +72,10 @@
 
 
 def kv_kernel(ids_ref, *refs):
-    wk_hbm, wv_hbm, fw_ref, bias_ref, kv_ref, toks_ref, wk_ref, wv_ref, sems, parts_ref = refs[8:]
+    wk_hbm, wv_hbm, fw_ref, bias_ref, kv_ref, toks_ref, wk_ref, wv_ref, sems, parts_ref = refs[PIECES:]
     y, c = ids_ref[2], ids_ref[3]
     weights = [(wk_hbm, wk_ref), (wv_hbm, wv_ref)]
-    toks_copies, weight_copies = fetch(ids_ref, refs[:8], toks_ref, weights, sems)
+    toks_copies, weight_copies = fetch(ids_ref, refs[:PIECES], toks_ref, weights, sems)
     wait_all(toks_copies)
     toks = toks_ref[...]
     logits = lax.dot_general(
@@ -120,8 +122,8 @@
 
 
 def query_kernel(ids_ref, *refs):
-    wq_hbm, same_ref, other_ref, toks_ref, wq_ref, sems = refs[8:]
-    toks_copies, weight_copies = fetch(ids_ref, refs[:8], toks_ref, [(wq_hbm, wq_ref)], sems)
+    wq_hbm, same_ref, other_ref, toks_ref, wq_ref, sems = refs[PIECES:]
+    toks_copies, weight_copies = fetch(ids_ref, refs[:PIECES], toks_ref, [(wq_hbm, wq_ref)], sems)
     wait_all(toks_copies + weight_copies)
     queries = jnp.dot(toks_ref[...], wq_ref[...], preferred_element_type=F32)
     same, other = by_parity(ids_ref, queries * HEAD_DIM**-0.5)
@@ -130,8 +132,8 @@
 
 
 def gate_kernel(ids_ref, *refs):
-    wg_hbm, gate_ref, toks_ref, wg_ref, sems = refs[8:]
-    toks_copies, weight_copies = fetch(ids_ref, refs[:8], toks_ref, [(wg_hbm, wg_ref)], sems)
+    wg_hbm, gate_ref, toks_ref, wg_ref, sems = refs[PIECES:]
+    toks_copies, weight_copies = fetch(ids_ref, refs[:PIECES], toks_ref, [(wg_hbm, wg_ref)], sems)
     wait_all(toks_copies + weight_copies)
     pre = jnp.dot(toks_ref[...], wg_ref[...], preferred_element_type=F32)
     gate_ref[0], gate_ref[1] = by_parity(ids_ref, 1.0 / (1.0 + jnp.exp(-pre)))
@@ -403,18 +405,23 @@
 def body(tokens, wq, wk, wv, wg, fw, fbias, wo):
     ids = jnp.stack([lax.axis_index(a) for a in AXES]).astype(jnp.int32)
 
-    near = [tokens] + [lax.ppermute(tokens, "y", ring(NY, s)) for s in (1, 2, 3)]
-    far = [lax.ppermute(near[0], "c", ring(NC, 1))]
-    far += [lax.ppermute(t, "c", ring(NC, 1)) for t in near[1:]]
+    top = PIECE // 2
+    direct = lax.ppermute(tokens[:top], "y", ring(NY, 2))
+    left = lax.ppermute(tokens, "y", ring(NY, 1))
+    right = lax.ppermute(tokens, "y", ring(NY, 3))
+    mate = lax.ppermute(tokens, "c", ring(NC, 1))
+    relayed = lax.ppermute(left[top:], "y", ring(NY, 1))
+    near = [tokens, left, right, direct, relayed]
+    far = [mate] + [lax.ppermute(t, "c", ring(NC, 1)) for t in near[1:]]
     flops = 2 * BLOCK * WIDTH * COLS
     hbm = pl.BlockSpec(memory_space=pltpu.HBM)
     weight = VMEM((WIDTH, COLS), BF)
 
     def project(kernel, outs, weights, extra=(), specs=(), scratch=()):
         return call(
-            kernel, outs, [sspec()] + [hbm] * (8 + len(weights)) + list(specs),
+            kernel, outs, [sspec()] + [hbm] * (PIECES + len(weights)) + list(specs),
             flops * len(weights),
-            [VMEM((BLOCK, WIDTH), BF), *[weight] * len(weights), pltpu.SemaphoreType.DMA((16,))]
+            [VMEM((BLOCK, WIDTH), BF), *[weight] * len(weights), pltpu.SemaphoreType.DMA((18,))]
             + list(scratch),
             mib=60,
         )(ids, *near, *far, *weights, *extra)

time: 140 us -> 140 us (level)
    ppermute x7 -> x9, waiting for transfers between devices: 11.2 us -> 8.68 us  [the longest x1 3.27 us: body(): left = lax.ppermute(tokens, 'y', ring(NY, 1))]
    ppermute x6, waiting for transfers between devices: 5.81 us -> 7.54 us  [swap(): out.append(lax.ppermute(values[s], 'x', ring(NX, s)))]
    ppermute x7 -> x9, starting transfers between devices: 6.33 us -> 7.43 us  [the longest x1 2.07 us: body(): direct = lax.ppermute(tokens[:top], 'y', ring(NY, 2))]
    unnamed x24 -> x28, local copies, waits for them, and re-layouts: 6.04 us -> 6.12 us
  transfers between devices with their start and end apart: 21 -> 23, of which waited for: 10 -> 10; matrix products, arithmetic and copies ran while one was open for 0% -> 1% of each run, Pallas kernels for 23% -> 23%
where the time goes in v3:
time: 140 us
  Pallas kernels  44.6 us (32%)
  waiting for transfers between devices  37.8 us (27%)
  blocking collectives  24.8 us (18%)
  starting transfers between devices  24.4 us (17%)
  local copies, waits for them, and re-layouts  7.11 us (5%)
    ppermute x8, waiting for transfers between devices, hop(): return lax.ppermute(value, 'z', ring(NZ, direction))  21.6 us
    pallas_call x3, Pallas kernels, body(): attention(functools.partial(step_kernel, s), STATE, 7, {4: 0, 5: 1, 6: 2})  20.4 us
    all_to_all x1, blocking collectives, body(): kv = lax.all_to_all(kvx, 'x', 0, 0, tiled=True)  14.3 us
    pallas_call x3, Pallas kernels, project(): call(kernel, outs, [sspec()] + [hbm] * (PIECES + len(weights)) + list(spe...  13.9 us
    all_to_all x1, blocking collectives, body(): rows = lax.all_to_all(att, ('y', 'c'), 0, 0, tiled=True)  10.6 us
    ppermute x8, starting transfers between devices, hop(): return lax.ppermute(value, 'z', ring(NZ, direction))  10.3 us
    ppermute x6, waiting for transfers between devices, swap(): out.append(lax.ppermute(values[s], 'x', ring(NX, s)))  7.54 us
    ppermute x6, starting transfers between devices, swap(): out.append(lax.ppermute(values[s], 'x', ring(NX, s)))  6.63 us
  transfers between devices with their start and end apart: 23, of which 10 were waited for; matrix products, arithmetic and copies ran while one was open for 1% of the time, Pallas kernels for 23%

profile of v3, /device:TPU:224, one launch (start us, length us, event | category | flops | bytes accessed | tf_op | source)
XLA Modules:
  0.0 139.6 jit_solution(358996861810462134)
XLA Ops:
  0.0 1.6 %collective-permute-start = (bf16[64,2048]{1,0:T(8,128)(2,1)}, bf16[64,2048]{1,0:T(8,128)(2,1)S(1)}, u32[]{:S(2)}, u32[]{:S(2)}) collective-permute-start(bf16[64,2048]{1,0:T(8,128)(2,1)} %refs_0_.5), channel_id=1, source_target_pairs={{0,2},{2,4},{4,6},{6,0},{1,3},{3,5},{5,7},{7,1},{8,10},{10,12},{12... | collective-permute-start | bytes 786440 | tf_op jit(solution)/shard_map/ppermute | solution.py:410
  1.6 1.7 %collective-permute-start.1 = (bf16[64,2048]{1,0:T(8,128)(2,1)}, bf16[64,2048]{1,0:T(8,128)(2,1)S(1)}, u32[]{:S(2)}, u32[]{:S(2)}) collective-permute-start(bf16[64,2048]{1,0:T(8,128)(2,1)} %refs_0_.5), channel_id=1, source_target_pairs={{0,6},{2,0},{4,2},{6,4},{1,7},{3,1},{5,3},{7,5},{8,14},{10,8},{12,... | collective-permute-start | bytes 786440 | tf_op jit(solution)/shard_map/ppermute | solution.py:411
  4.2 2.1 %collective-permute-start.2 = (bf16[32,2048]{1,0:T(8,128)(2,1)S(1)}, bf16[32,2048]{1,0:T(8,128)(2,1)S(1)}, u32[]{:S(2)}, u32[]{:S(2)}) collective-permute-start(bf16[32,2048]{1,0:T(8,128)(2,1)S(1)} %slice.12), channel_id=1, source_target_pairs={{0,4},{2,6},{4,0},{6,2},{1,5},{3,7},{5,1},{7,3},{8,12},{10,14},{12... | collective-permute-start | bytes 393224 | tf_op jit(solution)/shard_map/ppermute | solution.py:409
  6.3 3.3 %collective-permute-done.refs_1_ = bf16[64,2048]{1,0:T(8,128)(2,1)S(1)} collective-permute-done((bf16[64,2048]{1,0:T(8,128)(2,1)}, bf16[64,2048]{1,0:T(8,128)(2,1)S(1)}, u32[]{:S(2)}, u32[]{:S(2)}) %collective-permute-start) | collective-permute-done | bytes 262176 | tf_op jit(solution)/shard_map/ppermute | solution.py:410
  9.5 1.5 %collective-permute-start.3 = (bf16[32,2048]{1,0:T(8,128)(2,1)S(1)}, bf16[32,2048]{1,0:T(8,128)(2,1)S(1)}, u32[]{:S(2)}, u32[]{:S(2)}) collective-permute-start(bf16[32,2048]{1,0:T(8,128)(2,1)S(1)} %slice.16), channel_id=1, source_target_pairs={{0,2},{2,4},{4,6},{6,0},{1,3},{3,5},{5,7},{7,1},{8,10},{10,12},{12... | collective-permute-start | bytes 393224 | tf_op jit(solution)/shard_map/ppermute | solution.py:413
  11.7 3.0 %collective-permute-done.2.refs_3_ = bf16[32,2048]{1,0:T(8,128)(2,1)S(1)} collective-permute-done((bf16[32,2048]{1,0:T(8,128)(2,1)S(1)}, bf16[32,2048]{1,0:T(8,128)(2,1)S(1)}, u32[]{:S(2)}, u32[]{:S(2)}) %collective-permute-start.2) | collective-permute-done | bytes 131104 | tf_op jit(solution)/shard_map/ppermute | solution.py:409
  14.7 1.7 %collective-permute-done.3.refs_4_ = bf16[32,2048]{1,0:T(8,128)(2,1)S(1)} collective-permute-done((bf16[32,2048]{1,0:T(8,128)(2,1)S(1)}, bf16[32,2048]{1,0:T(8,128)(2,1)S(1)}, u32[]{:S(2)}, u32[]{:S(2)}) %collective-permute-start.3) | collective-permute-done | bytes 131104 | tf_op jit(solution)/shard_map/ppermute | solution.py:413
  18.6 5.7 %shard_map.83 = bf16[4,528,128]{2,1,0:T(8,128)(2,1)} custom-call(s32[4]{0:T(128)} %pad_add_fusion.ids_ref, bf16[64,2048]{1,0:T(8,128)(2,1)} %refs_0_.5, bf16[64,2048]{1,0:T(8,128)(2,1)} %copy-done.5, bf16[64,2048]{1,0:T(8,128)(2,1)} %copy-done.6, bf16[32,2048]{1,0:T(8,128)(2,1)} %copy-done.10, bf16[32,2048]{1,0:T(8,128)(2,1)} %copy-done.11, ...), custom_call_target="tpu_custom_call" | custom-call | flops 1073741824 | bytes 2097152 | tf_op jit(solution)/shard_map/pallas_call | solution.py:421
  24.3 14.3 %all_to_all.10.kv_ref = bf16[4,528,128]{2,1,0:T(8,128)(2,1)S(1)} all-to-all(bf16[4,528,128]{2,1,0:T(8,128)(2,1)} %shard_map.83), channel_id=1, replica_groups=mesh['z'=8,'x'=4,'y'=4,'c'=2] {'x'}, dimensions={0} | all-to-all | bytes 1081344 | tf_op jit(solution)/shard_map/all_to_all | solution.py:433
  38.5 2.0 %collective-permute-start.16 = (bf16[4,528,128]{2,1,0:T(8,128)(2,1)S(1)}, bf16[4,528,128]{2,1,0:T(8,128)(2,1)S(1)}, u32[]{:S(2)}, u32[]{:S(2)}) collective-permute-start(bf16[4,528,128]{2,1,0:T(8,128)(2,1)S(1)} %all_to_all.10.kv_ref), channel_id=1, source_target_pairs={{0,224},{32,0},{64,32},{96,64},{128,96},{160,128},{192,160},{224,1... | collective-permute-start | bytes 1622024 | tf_op jit(solution)/shard_map/ppermute | solution.py:446
  40.6 11.2 %collective-permute-done.12.front_ref = bf16[4,528,128]{2,1,0:T(8,128)(2,1)S(1)} collective-permute-done((bf16[4,528,128]{2,1,0:T(8,128)(2,1)S(1)}, bf16[4,528,128]{2,1,0:T(8,128)(2,1)S(1)}, u32[]{:S(2)}, u32[]{:S(2)}) %collective-permute-start.12) | collective-permute-done | bytes 540704 | tf_op jit(solution)/shard_map/ppermute | solution.py:446
  51.7 1.5 %collective-permute-start.13 = (bf16[4,528,128]{2,1,0:T(8,128)(2,1)S(1)}, bf16[4,528,128]{2,1,0:T(8,128)(2,1)S(1)}, u32[]{:S(2)}, u32[]{:S(2)}) collective-permute-start(bf16[4,528,128]{2,1,0:T(8,128)(2,1)S(1)} %collective-permute-done.12.front_ref), channel_id=1, source_target_pairs={{0,32},{32,64},{64,96},{96,128},{128,160},{160,192},{192,224},{224... | collective-permute-start | bytes 1622024 | tf_op jit(solution)/shard_map/ppermute | solution.py:446
  53.8 10.4 %collective-permute-done.13.front_ref = bf16[4,528,128]{2,1,0:T(8,128)(2,1)S(1)} collective-permute-done((bf16[4,528,128]{2,1,0:T(8,128)(2,1)S(1)}, bf16[4,528,128]{2,1,0:T(8,128)(2,1)S(1)}, u32[]{:S(2)}, u32[]{:S(2)}) %collective-permute-start.13) | collective-permute-done | bytes 540704 | tf_op jit(solution)/shard_map/ppermute | solution.py:446
  64.2 2.9 %collective-permute-start.14 = (bf16[4,528,128]{2,1,0:T(8,128)(2,1)S(1)}, bf16[4,528,128]{2,1,0:T(8,128)(2,1)S(1)}, u32[]{:S(2)}, u32[]{:S(2)}) collective-permute-start(bf16[4,528,128]{2,1,0:T(8,128)(2,1)S(1)} %collective-permute-done.13.front_ref), channel_id=1, source_target_pairs={{0,32},{32,64},{64,96},{96,128},{128,160},{160,192},{192,224},{224... | collective-permute-start | bytes 1622024 | tf_op jit(solution)/shard_map/ppermute | solution.py:446
  67.1 4.1 %shard_map.82 = (bf16[512,128]{1,0:T(8,128)(2,1)}, bf16[512,128]{1,0:T(8,128)(2,1)}) custom-call(s32[4]{0:T(128)} %pad_add_fusion.ids_ref, bf16[64,2048]{1,0:T(8,128)(2,1)} %refs_0_.5, bf16[64,2048]{1,0:T(8,128)(2,1)} %copy-done.5, bf16[64,2048]{1,0:T(8,128)(2,1)} %copy-done.6, bf16[32,2048]{1,0:T(8,128)(2,1)} %copy-done.10, bf16[32,2048]{1,0:T(8,128)(2,1)} %copy-done.11, ...), custom_call_target="tpu_custom_call" | custom-call | flops 536870912 | bytes 2097152 | tf_op jit(solution)/shard_map/pallas_call | solution.py:421
  71.1 1.1 collective-permute-start.10
  72.3 2.2 %collective-permute-start.11 = (bf16[512,128]{1,0:T(8,128)(2,1)}, bf16[512,128]{1,0:T(8,128)(2,1)S(1)}, u32[]{:S(2)}, u32[]{:S(2)}) collective-permute-start(bf16[512,128]{1,0:T(8,128)(2,1)} %get-tuple-element.25), channel_id=1, source_target_pairs={{0,24},{8,0},{16,8},{24,16},{1,25},{9,1},{17,9},{25,17},{2,26},{10... | collective-permute-start | bytes 393224 | tf_op jit(solution)/shard_map/ppermute | solution.py:439
  74.5 3.5 %collective-permute-done.10.q2 = bf16[512,128]{1,0:T(8,128)(2,1)S(1)} collective-permute-done((bf16[512,128]{1,0:T(8,128)(2,1)}, bf16[512,128]{1,0:T(8,128)(2,1)S(1)}, u32[]{:S(2)}, u32[]{:S(2)}) %collective-permute-start.10) | collective-permute-done | bytes 131104 | tf_op jit(solution)/shard_map/ppermute | solution.py:439
  78.0 2.8 %collective-permute-done.9.q1 = bf16[512,128]{1,0:T(8,128)(2,1)S(1)} collective-permute-done((bf16[512,128]{1,0:T(8,128)(2,1)}, bf16[512,128]{1,0:T(8,128)(2,1)S(1)}, u32[]{:S(2)}, u32[]{:S(2)}) %collective-permute-start.9) | collective-permute-done | bytes 131104 | tf_op jit(solution)/shard_map/ppermute | solution.py:439
  81.8 3.0 %shard_map.84 = (bf16[2048,256]{1,0:T(8,128)(2,1)S(1)}, f32[2,8,128]{2,1,0:T(8,128)S(1)}, f32[2,4,8,512]{3,2,1,0:T(8,128)S(1)}, f32[2,4,144,512]{3,2,1,0:T(8,128)S(1)}) custom-call(s32[4]{0:T(128)S(1)} %copy-done.2, bf16[512,128]{1,0:T(8,128)(2,1)S(1)} %copy-done.4, bf16[512,128]{1,0:T(8,128)(2,1)S(1)} %collective-permute-done.9.q1, ...), custom_call_target="tpu_custom_call" | custom-call | flops 1073741824 | bytes 2097152 | tf_op jit(solution)/shard_map/pallas_call | solution.py:455
  84.8 3.3 %collective-permute-start.15 = (bf16[2,528,128]{2,1,0:T(8,128)(2,1)S(1)}, bf16[2,528,128]{2,1,0:T(8,128)(2,1)S(1)}, u32[]{:S(2)}, u32[]{:S(2)}) collective-permute-start(bf16[2,528,128]{2,1,0:T(8,128)(2,1)S(1)} %slice.17), channel_id=1, source_target_pairs={{0,32},{32,64},{64,96},{96,128},{128,160},{160,192},{192,224},{224... | collective-permute-start | bytes 811016 | tf_op jit(solution)/shard_map/ppermute | solution.py:446
  88.2 6.8 %shard_map.85 = (f32[2,8,128]{2,1,0:T(8,128)S(1)}, f32[2,4,8,512]{3,2,1,0:T(8,128)S(1)}, f32[2,4,144,512]{3,2,1,0:T(8,128)S(1)}) custom-call(s32[4]{0:T(128)S(1)} %copy-done.2, bf16[2048,256]{1,0:T(8,128)(2,1)S(1)} %get-tuple-element.26.qa_ref, ...), custom_call_target="tpu_custom_call", output_to_operand_aliasing={{0}: (4, {}), {1}: (5, {}), {2}: (6, {})} | custom-call | flops 1073741824 | bytes 2097152 | tf_op jit(solution)/shard_map/pallas_call | solution.py:457
  95.0 6.8 %shard_map.86 = (f32[2,8,128]{2,1,0:T(8,128)S(1)}, f32[2,4,8,512]{3,2,1,0:T(8,128)S(1)}, f32[2,4,144,512]{3,2,1,0:T(8,128)S(1)}) custom-call(s32[4]{0:T(128)S(1)} %copy-done.2, bf16[2048,256]{1,0:T(8,128)(2,1)S(1)} %get-tuple-element.26.qa_ref, ...), custom_call_target="tpu_custom_call", output_to_operand_aliasing={{0}: (4, {}), {1}: (5, {}), {2}: (6, {})} | custom-call | flops 1073741824 | bytes 2097152 | tf_op jit(solution)/shard_map/pallas_call | solution.py:457
  101.9 6.8 %shard_map.87 = (f32[2,8,128]{2,1,0:T(8,128)S(1)}, f32[2,4,8,512]{3,2,1,0:T(8,128)S(1)}, f32[2,4,144,512]{3,2,1,0:T(8,128)S(1)}) custom-call(s32[4]{0:T(128)S(1)} %copy-done.2, bf16[2048,256]{1,0:T(8,128)(2,1)S(1)} %get-tuple-element.26.qa_ref, ...), custom_call_target="tpu_custom_call", output_to_operand_aliasing={{0}: (4, {}), {1}: (5, {}), {2}: (6, {})} | custom-call | flops 1073741824 | bytes 2097152 | tf_op jit(solution)/shard_map/pallas_call | solution.py:457
  108.7 4.2 %shard_map.88 = (bf16[528,128]{1,0:T(8,128)(2,1)S(1)}, bf16[528,128]{1,0:T(8,128)(2,1)S(1)}, bf16[528,128]{1,0:T(8,128)(2,1)S(1)}, bf16[528,128]{1,0:T(8,128)(2,1)S(1)}) custom-call(s32[4]{0:T(128)S(1)} %copy-done.2, bf16[2048,256]{1,0:T(8,128)(2,1)S(1)} %get-tuple-element.26.qa_ref, bf16[2,528,128]{2,1,0:T(8,128)(2,1)S(1)} %collective-permute-done.15.kv0_ref, ...), custom_call_target="tpu_custom_call" | custom-call | flops 1073741824 | bytes 2097152 | tf_op jit(solution)/shard_map/pallas_call | solution.py:460
  113.0 1.5 %collective-permute-start.21 = (bf16[528,128]{1,0:T(8,128)(2,1)S(1)}, bf16[528,128]{1,0:T(8,128)(2,1)S(1)}, u32[]{:S(2)}, u32[]{:S(2)}) collective-permute-start(bf16[528,128]{1,0:T(8,128)(2,1)S(1)} %get-tuple-element.41), channel_id=1, source_target_pairs={{0,16},{8,24},{16,0},{24,8},{1,17},{9,25},{17,1},{25,9},{2,18},{10... | collective-permute-start | bytes 405512 | tf_op jit(solution)/shard_map/ppermute | solution.py:439
  114.5 1.8 %collective-permute-start.22 = (bf16[528,128]{1,0:T(8,128)(2,1)S(1)}, bf16[528,128]{1,0:T(8,128)(2,1)S(1)}, u32[]{:S(2)}, u32[]{:S(2)}) collective-permute-start(bf16[528,128]{1,0:T(8,128)(2,1)S(1)} %get-tuple-element.42), channel_id=1, source_target_pairs={{0,24},{8,0},{16,8},{24,16},{1,25},{9,1},{17,9},{25,17},{2,26},{10... | collective-permute-start | bytes 405512 | tf_op jit(solution)/shard_map/ppermute | solution.py:439
  116.2 4.2 %shard_map.89.gate_ref = f32[2,512,128]{2,1,0:T(8,128)} custom-call(s32[4]{0:T(128)} %pad_add_fusion.ids_ref, bf16[64,2048]{1,0:T(8,128)(2,1)} %refs_0_.5, bf16[64,2048]{1,0:T(8,128)(2,1)} %copy-done.5, bf16[64,2048]{1,0:T(8,128)(2,1)} %copy-done.6, bf16[32,2048]{1,0:T(8,128)(2,1)} %copy-done.10, bf16[32,2048]{1,0:T(8,128)(2,1)} %copy-done.11, ...), custom_call_target="tpu_custom_call" | custom-call | flops 536870912 | bytes 2097152 | tf_op jit(solution)/shard_map/pallas_call | solution.py:421
  121.6 1.0 copy-done.1
  123.4 10.6 %all_to_all.11.rows_ref = bf16[8,64,256]{2,1,0:T(8,128)(2,1)S(1)} all-to-all(bf16[8,64,256]{2,1,0:T(8,128)(2,1)S(1)} %shard_map.90), channel_id=1, replica_groups=mesh['z'=8,'x'=4,'y'=4,'c'=2] {'y','c'}, dimensions={0} | all-to-all | bytes 524288 | tf_op jit(solution)/shard_map/all_to_all | solution.py:469
  134.0 3.4 %copy-done = bf16[2048,2048]{1,0:T(8,128)(2,1)S(1)} copy-done((bf16[2048,2048]{1,0:T(8,128)(2,1)S(1)}, bf16[2048,2048]{1,0:T(8,128)(2,1)}, u32[]{:S(2)}) %copy-start) | copy-done | bytes 8388632
  137.4 2.3 %shard_map.91 = bf16[64,2048]{1,0:T(8,128)(2,1)} custom-call(bf16[8,64,256]{2,1,0:T(8,128)(2,1)S(1)} %all_to_all.11.rows_ref, bf16[2048,2048]{1,0:T(8,128)(2,1)S(1)} %copy-done), custom_call_target="tpu_custom_call" | custom-call | flops 536870912 | bytes 2097152 | tf_op jit(solution)/shard_map/pallas_call | solution.py:470
  (59 shorter events, 7.3 us)
Async XLA Ops:
  0.0 9.5 %collective-permute-start = (bf16[64,2048]{1,0:T(8,128)(2,1)}, bf16[64,2048]{1,0:T(8,128)(2,1)S(1)}, u32[]{:S(2)}, u32[]{:S(2)}) collective-permute-start(bf16[64,2048]{1,0:T(8,128)(2,1)} %refs_0_.5), channel_id=1, source_target_pairs={{0,2},{2,4},{4,6},{6,0},{1,3},{3,5},{5,7},{7,1},{8,10},{10,12},{12... | collective-permute-start | bytes 786440 | tf_op jit(solution)/shard_map/ppermute | solution.py:410
  1.6 10.0 %collective-permute-start.1 = (bf16[64,2048]{1,0:T(8,128)(2,1)}, bf16[64,2048]{1,0:T(8,128)(2,1)S(1)}, u32[]{:S(2)}, u32[]{:S(2)}) collective-permute-start(bf16[64,2048]{1,0:T(8,128)(2,1)} %refs_0_.5), channel_id=1, source_target_pairs={{0,6},{2,0},{4,2},{6,4},{1,7},{3,1},{5,3},{7,5},{8,14},{10,8},{12,... | collective-permute-start | bytes 786440 | tf_op jit(solution)/shard_map/ppermute | solution.py:411
  4.2 10.5 %collective-permute-start.2 = (bf16[32,2048]{1,0:T(8,128)(2,1)S(1)}, bf16[32,2048]{1,0:T(8,128)(2,1)S(1)}, u32[]{:S(2)}, u32[]{:S(2)}) collective-permute-start(bf16[32,2048]{1,0:T(8,128)(2,1)S(1)} %slice.12), channel_id=1, source_target_pairs={{0,4},{2,6},{4,0},{6,2},{1,5},{3,7},{5,1},{7,3},{8,12},{10,14},{12... | collective-permute-start | bytes 393224 | tf_op jit(solution)/shard_map/ppermute | solution.py:409
  9.5 8.2 %copy-start.5 = (bf16[64,2048]{1,0:T(8,128)(2,1)}, bf16[64,2048]{1,0:T(8,128)(2,1)S(1)}, u32[]{:S(2)}) copy-start(bf16[64,2048]{1,0:T(8,128)(2,1)S(1)} %collective-permute-done.refs_1_) | copy-start | bytes 786436
  9.5 6.8 %collective-permute-start.3 = (bf16[32,2048]{1,0:T(8,128)(2,1)S(1)}, bf16[32,2048]{1,0:T(8,128)(2,1)S(1)}, u32[]{:S(2)}, u32[]{:S(2)}) collective-permute-start(bf16[32,2048]{1,0:T(8,128)(2,1)S(1)} %slice.16), channel_id=1, source_target_pairs={{0,2},{2,4},{4,6},{6,0},{1,3},{3,5},{5,7},{7,1},{8,10},{10,12},{12... | collective-permute-start | bytes 393224 | tf_op jit(solution)/shard_map/ppermute | solution.py:413
  11.1 5.9 %collective-permute-start.4 = (bf16[64,2048]{1,0:T(8,128)(2,1)}, bf16[64,2048]{1,0:T(8,128)(2,1)S(1)}, u32[]{:S(2)}, u32[]{:S(2)}) collective-permute-start(bf16[64,2048]{1,0:T(8,128)(2,1)} %refs_0_.5), channel_id=1, source_target_pairs={{0,1},{1,0},{2,3},{3,2},{4,5},{5,4},{6,7},{7,6},{8,9},{9,8},{10,11... | collective-permute-start | bytes 786440 | tf_op jit(solution)/shard_map/ppermute | solution.py:412
  11.1 6.7 %collective-permute-start.5 = (bf16[64,2048]{1,0:T(8,128)(2,1)S(1)}, bf16[64,2048]{1,0:T(8,128)(2,1)S(1)}, u32[]{:S(2)}, u32[]{:S(2)}) collective-permute-start(bf16[64,2048]{1,0:T(8,128)(2,1)S(1)} %collective-permute-done.refs_1_), channel_id=1, source_target_pairs={{0,1},{1,0},{2,3},{3,2},{4,5},{5,4},{6,7},{7,6},{8,9},{9,8},{10,11... | collective-permute-start | bytes 786440 | tf_op jit(solution)/shard_map/ppermute | solution.py:415
  11.6 6.2 %copy-start.6 = (bf16[64,2048]{1,0:T(8,128)(2,1)}, bf16[64,2048]{1,0:T(8,128)(2,1)S(1)}, u32[]{:S(2)}) copy-start(bf16[64,2048]{1,0:T(8,128)(2,1)S(1)} %collective-permute-done.1.refs_2_) | copy-start | bytes 786436
  11.6 6.2 %collective-permute-start.6 = (bf16[64,2048]{1,0:T(8,128)(2,1)S(1)}, bf16[64,2048]{1,0:T(8,128)(2,1)S(1)}, u32[]{:S(2)}, u32[]{:S(2)}) collective-permute-start(bf16[64,2048]{1,0:T(8,128)(2,1)S(1)} %collective-permute-done.1.refs_2_), channel_id=1, source_target_pairs={{0,1},{1,0},{2,3},{3,2},{4,5},{5,4},{6,7},{7,6},{8,9},{9,8},{10,11... | collective-permute-start | bytes 786440 | tf_op jit(solution)/shard_map/ppermute | solution.py:415
  14.6 3.1 %copy-start.10 = (bf16[32,2048]{1,0:T(8,128)(2,1)}, bf16[32,2048]{1,0:T(8,128)(2,1)S(1)}, u32[]{:S(2)}) copy-start(bf16[32,2048]{1,0:T(8,128)(2,1)S(1)} %collective-permute-done.2.refs_3_) | copy-start | bytes 393220
  14.7 2.3 %collective-permute-start.7 = (bf16[32,2048]{1,0:T(8,128)(2,1)S(1)}, bf16[32,2048]{1,0:T(8,128)(2,1)S(1)}, u32[]{:S(2)}, u32[]{:S(2)}) collective-permute-start(bf16[32,2048]{1,0:T(8,128)(2,1)S(1)} %collective-permute-done.2.refs_3_), channel_id=1, source_target_pairs={{0,1},{1,0},{2,3},{3,2},{4,5},{5,4},{6,7},{7,6},{8,9},{9,8},{10,11... | collective-permute-start | bytes 393224 | tf_op jit(solution)/shard_map/ppermute | solution.py:415
  16.4 1.4 %copy-start.11 = (bf16[32,2048]{1,0:T(8,128)(2,1)}, bf16[32,2048]{1,0:T(8,128)(2,1)S(1)}, u32[]{:S(2)}) copy-start(bf16[32,2048]{1,0:T(8,128)(2,1)S(1)} %collective-permute-done.3.refs_4_) | copy-start | bytes 393220
  16.4 1.3 collective-permute-start.8
  24.3 56.6 %copy-start.2 = (s32[4]{0:T(128)S(1)}, s32[4]{0:T(128)}, u32[]{:S(2)}) copy-start(s32[4]{0:T(128)} %pad_add_fusion.ids_ref) | copy-start | bytes 52
  38.5 13.2 %collective-permute-start.12 = (bf16[4,528,128]{2,1,0:T(8,128)(2,1)S(1)}, bf16[4,528,128]{2,1,0:T(8,128)(2,1)S(1)}, u32[]{:S(2)}, u32[]{:S(2)}) collective-permute-start(bf16[4,528,128]{2,1,0:T(8,128)(2,1)S(1)} %all_to_all.10.kv_ref), channel_id=1, source_target_pairs={{0,32},{32,64},{64,96},{96,128},{128,160},{160,192},{192,224},{224... | collective-permute-start | bytes 1622024 | tf_op jit(solution)/shard_map/ppermute | solution.py:446
  38.5 14.7 %collective-permute-start.16 = (bf16[4,528,128]{2,1,0:T(8,128)(2,1)S(1)}, bf16[4,528,128]{2,1,0:T(8,128)(2,1)S(1)}, u32[]{:S(2)}, u32[]{:S(2)}) collective-permute-start(bf16[4,528,128]{2,1,0:T(8,128)(2,1)S(1)} %all_to_all.10.kv_ref), channel_id=1, source_target_pairs={{0,224},{32,0},{64,32},{96,64},{128,96},{160,128},{192,160},{224,1... | collective-permute-start | bytes 1622024 | tf_op jit(solution)/shard_map/ppermute | solution.py:446
  51.7 12.4 %collective-permute-start.13 = (bf16[4,528,128]{2,1,0:T(8,128)(2,1)S(1)}, bf16[4,528,128]{2,1,0:T(8,128)(2,1)S(1)}, u32[]{:S(2)}, u32[]{:S(2)}) collective-permute-start(bf16[4,528,128]{2,1,0:T(8,128)(2,1)S(1)} %collective-permute-done.12.front_ref), channel_id=1, source_target_pairs={{0,32},{32,64},{64,96},{96,128},{128,160},{160,192},{192,224},{224... | collective-permute-start | bytes 1622024 | tf_op jit(solution)/shard_map/ppermute | solution.py:446
  53.2 13.8 %collective-permute-start.17 = (bf16[4,528,128]{2,1,0:T(8,128)(2,1)S(1)}, bf16[4,528,128]{2,1,0:T(8,128)(2,1)S(1)}, u32[]{:S(2)}, u32[]{:S(2)}) collective-permute-start(bf16[4,528,128]{2,1,0:T(8,128)(2,1)S(1)} %collective-permute-done.16.back_ref), channel_id=1, source_target_pairs={{0,224},{32,0},{64,32},{96,64},{128,96},{160,128},{192,160},{224,1... | collective-permute-start | bytes 1622024 | tf_op jit(solution)/shard_map/ppermute | solution.py:446
  64.2 20.6 %collective-permute-start.14 = (bf16[4,528,128]{2,1,0:T(8,128)(2,1)S(1)}, bf16[4,528,128]{2,1,0:T(8,128)(2,1)S(1)}, u32[]{:S(2)}, u32[]{:S(2)}) collective-permute-start(bf16[4,528,128]{2,1,0:T(8,128)(2,1)S(1)} %collective-permute-done.13.front_ref), channel_id=1, source_target_pairs={{0,32},{32,64},{64,96},{96,128},{128,160},{160,192},{192,224},{224... | collective-permute-start | bytes 1622024 | tf_op jit(solution)/shard_map/ppermute | solution.py:446
  67.1 21.0 %collective-permute-start.18 = (bf16[4,528,128]{2,1,0:T(8,128)(2,1)S(1)}, bf16[4,528,128]{2,1,0:T(8,128)(2,1)S(1)}, u32[]{:S(2)}, u32[]{:S(2)}) collective-permute-start(bf16[4,528,128]{2,1,0:T(8,128)(2,1)S(1)} %collective-permute-done.17.back_ref), channel_id=1, source_target_pairs={{0,224},{32,0},{64,32},{96,64},{128,96},{160,128},{192,160},{224,1... | collective-permute-start | bytes 1622024 | tf_op jit(solution)/shard_map/ppermute | solution.py:446
  71.1 6.9 %collective-permute-start.10 = (bf16[512,128]{1,0:T(8,128)(2,1)}, bf16[512,128]{1,0:T(8,128)(2,1)S(1)}, u32[]{:S(2)}, u32[]{:S(2)}) collective-permute-start(bf16[512,128]{1,0:T(8,128)(2,1)} %get-tuple-element.24.q0), channel_id=1, source_target_pairs={{0,16},{8,24},{16,0},{24,8},{1,17},{9,25},{17,1},{25,9},{2,18},{10... | collective-permute-start | bytes 393224 | tf_op jit(solution)/shard_map/ppermute | solution.py:439
  72.3 5.8 %collective-permute-start.11 = (bf16[512,128]{1,0:T(8,128)(2,1)}, bf16[512,128]{1,0:T(8,128)(2,1)S(1)}, u32[]{:S(2)}, u32[]{:S(2)}) collective-permute-start(bf16[512,128]{1,0:T(8,128)(2,1)} %get-tuple-element.25), channel_id=1, source_target_pairs={{0,24},{8,0},{16,8},{24,16},{1,25},{9,1},{17,9},{25,17},{2,26},{10... | collective-permute-start | bytes 393224 | tf_op jit(solution)/shard_map/ppermute | solution.py:439
  74.5 6.4 %collective-permute-start.9 = (bf16[512,128]{1,0:T(8,128)(2,1)}, bf16[512,128]{1,0:T(8,128)(2,1)S(1)}, u32[]{:S(2)}, u32[]{:S(2)}) collective-permute-start(bf16[512,128]{1,0:T(8,128)(2,1)} %get-tuple-element.25), channel_id=1, source_target_pairs={{0,8},{8,16},{16,24},{24,0},{1,9},{9,17},{17,25},{25,1},{2,10},{10... | collective-permute-start | bytes 393224 | tf_op jit(solution)/shard_map/ppermute | solution.py:439
  80.8 0.9 copy-start.4
  84.8 23.9 %collective-permute-start.15 = (bf16[2,528,128]{2,1,0:T(8,128)(2,1)S(1)}, bf16[2,528,128]{2,1,0:T(8,128)(2,1)S(1)}, u32[]{:S(2)}, u32[]{:S(2)}) collective-permute-start(bf16[2,528,128]{2,1,0:T(8,128)(2,1)S(1)} %slice.17), channel_id=1, source_target_pairs={{0,32},{32,64},{64,96},{96,128},{128,160},{160,192},{192,224},{224... | collective-permute-start | bytes 811016 | tf_op jit(solution)/shard_map/ppermute | solution.py:446
  88.1 20.6 %collective-permute-start.19 = (bf16[2,528,128]{2,1,0:T(8,128)(2,1)S(1)}, bf16[2,528,128]{2,1,0:T(8,128)(2,1)S(1)}, u32[]{:S(2)}, u32[]{:S(2)}) collective-permute-start(bf16[2,528,128]{2,1,0:T(8,128)(2,1)S(1)} %slice.18), channel_id=1, source_target_pairs={{0,224},{32,0},{64,32},{96,64},{128,96},{160,128},{192,160},{224,1... | collective-permute-start | bytes 811016 | tf_op jit(solution)/shard_map/ppermute | solution.py:446
  112.9 8.7 %copy-start.3 = (s32[4]{0:T(128)S(1)}, s32[4]{0:T(128)}, u32[]{:S(2)}) copy-start(s32[4]{0:T(128)} %pad_add_fusion.ids_ref) | copy-start | bytes 52
  112.9 7.7 %collective-permute-start.20 = (bf16[528,128]{1,0:T(8,128)(2,1)S(1)}, bf16[528,128]{1,0:T(8,128)(2,1)S(1)}, u32[]{:S(2)}, u32[]{:S(2)}) collective-permute-start(bf16[528,128]{1,0:T(8,128)(2,1)S(1)} %get-tuple-element.40), channel_id=1, source_target_pairs={{0,8},{8,16},{16,24},{24,0},{1,9},{9,17},{17,25},{25,1},{2,10},{10... | collective-permute-start | bytes 405512 | tf_op jit(solution)/shard_map/ppermute | solution.py:439
  113.0 7.7 %collective-permute-start.21 = (bf16[528,128]{1,0:T(8,128)(2,1)S(1)}, bf16[528,128]{1,0:T(8,128)(2,1)S(1)}, u32[]{:S(2)}, u32[]{:S(2)}) collective-permute-start(bf16[528,128]{1,0:T(8,128)(2,1)S(1)} %get-tuple-element.41), channel_id=1, source_target_pairs={{0,16},{8,24},{16,0},{24,8},{1,17},{9,25},{17,1},{25,9},{2,18},{10... | collective-permute-start | bytes 405512 | tf_op jit(solution)/shard_map/ppermute | solution.py:439
  114.5 7.1 %collective-permute-start.22 = (bf16[528,128]{1,0:T(8,128)(2,1)S(1)}, bf16[528,128]{1,0:T(8,128)(2,1)S(1)}, u32[]{:S(2)}, u32[]{:S(2)}) collective-permute-start(bf16[528,128]{1,0:T(8,128)(2,1)S(1)} %get-tuple-element.42), channel_id=1, source_target_pairs={{0,24},{8,0},{16,8},{24,16},{1,25},{9,1},{17,9},{25,17},{2,26},{10... | collective-permute-start | bytes 405512 | tf_op jit(solution)/shard_map/ppermute | solution.py:439
  121.6 1.0 copy-start.1
  134.0 3.4 %copy-start = (bf16[2048,2048]{1,0:T(8,128)(2,1)S(1)}, bf16[2048,2048]{1,0:T(8,128)(2,1)}, u32[]{:S(2)}) copy-start(bf16[2048,2048]{1,0:T(8,128)(2,1)} %wo_ref.1) | copy-start | bytes 25165828
  (5 other events, 3.8 us)
